TPU v7x, 256 devices: a 8x8x2 block of a 8x8x16 slice. The times are simulated.
256 devices in a mesh: grp: 2 (over z), kv: 16 (over y, core), tp: 8 (over x).
Axes of the slice: x: 8, y: 8, z: 2, core: 2. Of those that a mesh axis runs over, the one named last changes fastest.
The devices are a block of a 8x8x16 slice.
Arguments:
- tokens: bfloat16 [512, 4096], P('grp', ('kv', 'tp')), parts along dimension 0, may hold values from -20 to 20, as said below
- norm_gain: bfloat16 [4096], P('kv'), may hold values from 0.099609375 to 1.8984375
- w_query: bfloat16 [4096, 2048], P('kv', 'tp'), may hold values from -0.09375 to 0.09375
- w_key: bfloat16 [4096, 2048], P('kv', 'tp'), may hold values from -0.09375 to 0.09375
- w_value: bfloat16 [4096, 4096], P('kv', 'tp'), may hold values from -0.09375 to 0.09375
- w_outgate: bfloat16 [4096, 4096], P('kv', 'tp'), may hold values from -0.09375 to 0.09375
- w_input_gate: bfloat16 [4096, 32], P('kv'), may hold values from -0.09375 to 0.09375
- w_forget_gate: bfloat16 [4096, 32], P('kv'), may hold values from -0.09375 to 0.09375
- memory: float32 [512, 32, 64, 128], P(('grp', 'kv'), 'tp'), parts along dimension 0, may hold values from -4 to 4
- normalizer: float32 [512, 32, 64], P(('grp', 'kv'), 'tp'), parts along dimension 0, may hold values from -4 to 4
- stabilizer: float32 [512, 32], P(('grp', 'kv'), 'tp'), parts along dimension 0, may hold values from -4 to 4
- w_mix_out: bfloat16 [4096, 4096], P('tp', 'kv'), may hold values from -0.09375 to 0.09375
- ffn_gain: bfloat16 [4096], P('kv'), may hold values from 0.099609375 to 1.8984375
- w_gate: bfloat16 [4096, 11264], P('kv', 'tp'), may hold values from -0.09375 to 0.09375
- w_up: bfloat16 [4096, 11264], P('kv', 'tp'), may hold values from -0.09375 to 0.09375
- w_down: bfloat16 [11264, 4096], P('tp', 'kv'), may hold values from -0.3125 to 0.3125
Outputs:
- layer_out: bfloat16 [512, 4096], P('grp', ('kv', 'tp')), parts along dimension 0
- new_memory: float32 [512, 32, 64, 128], P(('grp', 'kv'), 'tp'), parts along dimension 0
- new_normalizer: float32 [512, 32, 64], P(('grp', 'kv'), 'tp'), parts along dimension 0
- new_stabilizer: float32 [512, 32], P(('grp', 'kv'), 'tp'), parts along dimension 0
There are 2 independent parts, one for each index of `grp`. A program takes and returns all parts, laid end to end along the dimension named above; an argument that names none is the same for every part. Nothing has to cross between parts.
Inputs may be any that keep to these rules, and one draw needn't show every extreme that they name: tokens' feature scales differ by column and by sequence.
All inputs are finite; a program needn't handle non-finite values.
Results may differ from a plain program's by a relative error of at most 0.029.
Values may be sent and summed in bfloat16 or wider, within the bound.
A program may use at most 64 MiB of HBM per device.

v0:
```python
import jax
import jax.numpy as jnp
from jax import lax
from jax.sharding import PartitionSpec as P

D = 4096
DQK = 64
DV = 128


def copy_for_each(array, axis):
    count = lax.axis_size(axis)
    return lax.all_to_all(
        jnp.broadcast_to(array[None], (count, *array.shape)), axis, 0, 0, tiled=True
    )


def laid_out(pieces, dim):
    lengths = list(pieces.shape[1:])
    lengths[dim] *= pieces.shape[0]
    return jnp.moveaxis(pieces, 0, dim).reshape(lengths)


def gather_directly(array, axis, dim):
    pieces = copy_for_each(array, axis)
    return laid_out(pieces, dim)


def split_up(array, dim, count):
    before, after = (array.shape[:dim], array.shape[dim + 1 :])
    return jnp.moveaxis(array.reshape(*before, count, -1, *after), dim, 0)


def summed_on_arrival(array, axis, dim):
    count = lax.axis_size(axis)
    pieces = lax.all_to_all(split_up(array, dim, count), axis, 0, 0, tiled=True)
    return jnp.sum(pieces, axis=0)


def sum_at_owner(array, axis, dim):
    count = lax.axis_size(axis)
    pieces = lax.all_to_all(split_up(array, dim, count), axis, 0, 0, tiled=True)
    return jnp.sum(pieces.astype(jnp.float32), axis=0)


def in_one_piece(arrays, axis, dim, along):
    ends, at = ([], 0)
    for a in arrays[:-1]:
        at += a.shape[along]
        ends.append(at)
    both = jnp.concatenate(arrays, axis=along)
    return tuple(
        jnp.split(lax.psum_scatter(both, axis, scatter_dimension=dim, tiled=True), ends, axis=along)
    )


def over_copies(array, axis):
    return copy_for_each(array, axis).sum(axis=0)


def shards(
    tokens,
    norm_gain,
    w_query,
    w_key,
    w_value,
    w_outgate,
    w_input_gate,
    w_forget_gate,
    memory,
    normalizer,
    stabilizer,
    w_mix_out,
    ffn_gain,
    w_gate,
    w_up,
    w_down,
):
    seqs = tokens.shape[0]
    weights = (w_query, w_key, w_value, w_outgate, w_input_gate, w_forget_gate)
    start_proj = tuple((jnp.zeros((seqs, weight.shape[1]), jnp.float32) for weight in weights))
    start_proj = start_proj + (jnp.zeros((seqs,), jnp.float32),)
    wide = gather_directly(tokens, "tp", 1).astype(jnp.float32)
    gain = norm_gain.astype(jnp.float32)
    normed = (wide * gain[None, :]).astype(jnp.bfloat16)
    sums = tuple(
        (jnp.dot(normed, weight, preferred_element_type=jnp.float32) for weight in weights)
    )
    totals = sums + (jnp.sum(wide * wide, axis=1),)
    z_query, z_key, z_value, z_outgate, z_input, z_forget, squares = jax.tree.map(
        lambda part: summed_on_arrival(part, "kv", 0), totals
    )
    own = z_query.shape[0]
    local_heads = memory.shape[1]
    scale1 = lax.rsqrt(squares / D + 1e-06)
    head_start = lax.axis_index("tp") * local_heads
    query = (scale1[:, None] * z_query).reshape(own, local_heads, DQK) * DQK ** (-0.5)
    key = (scale1[:, None] * z_key).reshape(own, local_heads, DQK)
    value = (scale1[:, None] * z_value).reshape(own, local_heads, DV)
    outgate = scale1[:, None] * z_outgate
    igate = scale1[:, None] * lax.dynamic_slice_in_dim(z_input, head_start, local_heads, 1)
    lforget = jax.nn.log_sigmoid(
        scale1[:, None] * lax.dynamic_slice_in_dim(z_forget, head_start, local_heads, 1)
    )
    new_stabilizer = jnp.maximum(lforget + stabilizer, igate)
    decay = jnp.exp(lforget + stabilizer - new_stabilizer)
    inflow = jnp.exp(igate - new_stabilizer)
    new_memory = (
        decay[:, :, None, None] * memory
        + inflow[:, :, None, None] * key[:, :, :, None] * value[:, :, None, :]
    )
    new_normalizer = decay[:, :, None] * normalizer + inflow[:, :, None] * key
    numer = jnp.einsum("bhd,bhde->bhe", query, new_memory)
    denom = jnp.sum(query * new_normalizer, axis=-1)
    readout = numer / jnp.maximum(jnp.abs(denom), jnp.exp(-new_stabilizer))[:, :, None]
    gated = (jax.nn.sigmoid(outgate) * readout.reshape(own, local_heads * DV)).astype(jnp.bfloat16)
    mix_partial = jnp.dot(
        gather_directly(gated, "kv", 0), w_mix_out, preferred_element_type=jnp.float32
    )
    mix_total = sum_at_owner(mix_partial.astype(jnp.bfloat16), "tp", 1)
    mixed_in = (tokens.astype(jnp.float32) + mix_total).astype(jnp.bfloat16)
    wide = gather_directly(mixed_in, "tp", 1).astype(jnp.float32)
    gain = ffn_gain.astype(jnp.float32)
    normed = (wide * gain[None, :]).astype(jnp.bfloat16)
    gate_sum = jnp.dot(normed, w_gate, preferred_element_type=jnp.float32)
    up_sum = jnp.dot(normed, w_up, preferred_element_type=jnp.float32)
    square_part = jnp.sum(wide * wide, axis=1)
    gate_share, up_share = in_one_piece((gate_sum, up_sum), "kv", 1, 0)
    square_sum = over_copies(square_part, "kv")
    scale2 = lax.rsqrt(square_sum / D + 1e-06)[:, None]
    hidden_share = (jax.nn.silu(scale2 * gate_share) * (scale2 * up_share)).astype(jnp.bfloat16)
    down_partial = jnp.dot(
        lax.all_gather(hidden_share, "kv", axis=1, tiled=True),
        w_down,
        preferred_element_type=jnp.float32,
    )
    down_total = sum_at_owner(down_partial.astype(jnp.bfloat16), "tp", 1)
    layer_out = (mixed_in.astype(jnp.float32) + down_total).astype(jnp.bfloat16)
    return (layer_out, new_memory, new_normalizer, new_stabilizer)


def solution(mesh):
    in_specs = (
        P("grp", ("kv", "tp")),
        P("kv"),
        P("kv", "tp"),
        P("kv", "tp"),
        P("kv", "tp"),
        P("kv", "tp"),
        P("kv", None),
        P("kv", None),
        P(("grp", "kv"), "tp", None, None),
        P(("grp", "kv"), "tp", None),
        P(("grp", "kv"), "tp"),
        P("tp", "kv"),
        P("kv"),
        P("kv", "tp"),
        P("kv", "tp"),
        P("tp", "kv"),
    )
    out_specs = (
        P("grp", ("kv", "tp")),
        P(("grp", "kv"), "tp", None, None),
        P(("grp", "kv"), "tp", None),
        P(("grp", "kv"), "tp"),
    )
    return jax.shard_map(shards, mesh=mesh, in_specs=in_specs, out_specs=out_specs, check_vma=False)
```

profile of v0, /device:TPU:513, one launch (start us, length us, event | category | flops | bytes accessed | tf_op | source)
XLA Modules:
  0.0 294.8 jit_solution(17293236000279843596)
XLA Ops:
  7.2 1.5 broadcast_in_dim.8
  8.7 7.9 %all-to-all-start = ((bf16[8,256,32]{1,2,0:T(8,128)(2,1)}), bf16[8,256,32]{1,2,0:T(8,128)(2,1)S(1)}, u32[]{:S(2)}, u32[]{:S(2)}) async-start(bf16[8,256,32]{1,2,0:T(8,128)(2,1)} %broadcast_in_dim.8), calls=%async_computation | async-start | bytes 262144 | tf_op jit(solution)/shard_map/all_to_all | solution.py:13
  17.2 7.3 %all-to-all-done = bf16[8,256,32]{1,2,0:T(8,128)(2,1)S(1)} async-done(((bf16[8,256,32]{1,2,0:T(8,128)(2,1)}), bf16[8,256,32]{1,2,0:T(8,128)(2,1)S(1)}, u32[]{:S(2)}, u32[]{:S(2)}) %all-to-all-start) | async-done | bytes 131104 | tf_op jit(solution)/shard_map/all_to_all | solution.py:13
  25.2 20.3 %all-to-all-start.1 = ((f32[16,1,16]{2,1,0:T(1,128)}), f32[16,1,16]{2,1,0:T(1,128)S(1)}, u32[]{:S(2)}, u32[]{:S(2)}) async-start(f32[16,1,16]{2,1,0:T(1,128)} %all_to_all.44), calls=%async_computation.1 | async-start | bytes 16384 | tf_op jit(solution)/shard_map/all_to_all | solution.py:36
  47.3 5.3 %all-to-all-done.1 = f32[16,1,16]{2,1,0:T(1,128)S(1)} async-done(((f32[16,1,16]{2,1,0:T(1,128)}), f32[16,1,16]{2,1,0:T(1,128)S(1)}, u32[]{:S(2)}, u32[]{:S(2)}) %all-to-all-start.1) | async-done | bytes 1056 | tf_op jit(solution)/shard_map/all_to_all | solution.py:36
  52.6 4.0 %all-to-all-start.5 = ((f32[16,1,512]{2,1,0:T(1,128)}), f32[16,1,512]{2,1,0:T(1,128)S(1)}, u32[]{:S(2)}, u32[]{:S(2)}) async-start(f32[16,1,512]{2,1,0:T(1,128)} %reshape.179), calls=%async_computation.5 | async-start | bytes 65536 | tf_op jit(solution)/shard_map/all_to_all | solution.py:36
  57.5 6.7 %all-to-all-done.5 = f32[16,1,512]{2,1,0:T(1,128)S(1)} async-done(((f32[16,1,512]{2,1,0:T(1,128)}), f32[16,1,512]{2,1,0:T(1,128)S(1)}, u32[]{:S(2)}, u32[]{:S(2)}) %all-to-all-start.5) | async-done | bytes 32800 | tf_op jit(solution)/shard_map/all_to_all | solution.py:36
  64.2 3.7 %all-to-all-start.4 = ((f32[16,1,512]{2,1,0:T(1,128)}), f32[16,1,512]{2,1,0:T(1,128)S(1)}, u32[]{:S(2)}, u32[]{:S(2)}) async-start(f32[16,1,512]{2,1,0:T(1,128)} %reshape.181), calls=%async_computation.4 | async-start | bytes 65536 | tf_op jit(solution)/shard_map/all_to_all | solution.py:36
  68.8 6.7 %all-to-all-done.4 = f32[16,1,512]{2,1,0:T(1,128)S(1)} async-done(((f32[16,1,512]{2,1,0:T(1,128)}), f32[16,1,512]{2,1,0:T(1,128)S(1)}, u32[]{:S(2)}, u32[]{:S(2)}) %all-to-all-start.4) | async-done | bytes 32800 | tf_op jit(solution)/shard_map/all_to_all | solution.py:36
  75.5 3.7 %all-to-all-start.6 = ((f32[16,16,256]{2,1,0:T(8,128)}), f32[16,16,256]{2,1,0:T(8,128)S(1)}, u32[]{:S(2)}, u32[]{:S(2)}) async-start(f32[16,16,256]{2,1,0:T(8,128)} %fusion.6), calls=%async_computation.6 | async-start | bytes 524288 | tf_op jit(solution)/shard_map/all_to_all | solution.py:36
  80.3 11.0 %all-to-all-done.6 = f32[16,16,256]{2,1,0:T(8,128)S(1)} async-done(((f32[16,16,256]{2,1,0:T(8,128)}), f32[16,16,256]{2,1,0:T(8,128)S(1)}, u32[]{:S(2)}, u32[]{:S(2)}) %all-to-all-start.6) | async-done | bytes 262176 | tf_op jit(solution)/shard_map/all_to_all | solution.py:36
  91.2 3.7 %all-to-all-start.3 = ((f32[16,16,256]{2,1,0:T(8,128)}), f32[16,16,256]{2,1,0:T(8,128)S(1)}, u32[]{:S(2)}, u32[]{:S(2)}) async-start(f32[16,16,256]{2,1,0:T(8,128)} %fusion.8), calls=%async_computation.3 | async-start | bytes 524288 | tf_op jit(solution)/shard_map/all_to_all | solution.py:36
  95.0 1.0 fusion.2
  97.0 8.6 %all-to-all-done.3 = f32[16,16,256]{2,1,0:T(8,128)S(1)} async-done(((f32[16,16,256]{2,1,0:T(8,128)}), f32[16,16,256]{2,1,0:T(8,128)S(1)}, u32[]{:S(2)}, u32[]{:S(2)}) %all-to-all-start.3) | async-done | bytes 262176 | tf_op jit(solution)/shard_map/all_to_all | solution.py:36
  105.6 3.7 %all-to-all-start.7 = ((f32[16,16,512]{2,1,0:T(8,128)}), f32[16,16,512]{2,1,0:T(8,128)S(1)}, u32[]{:S(2)}, u32[]{:S(2)}) async-start(f32[16,16,512]{2,1,0:T(8,128)} %fusion.2), calls=%async_computation.7 | async-start | bytes 1048576 | tf_op jit(solution)/shard_map/all_to_all | solution.py:36
  112.8 12.8 %all-to-all-done.7 = f32[16,16,512]{2,1,0:T(8,128)S(1)} async-done(((f32[16,16,512]{2,1,0:T(8,128)}), f32[16,16,512]{2,1,0:T(8,128)S(1)}, u32[]{:S(2)}, u32[]{:S(2)}) %all-to-all-start.7) | async-done | bytes 524320 | tf_op jit(solution)/shard_map/all_to_all | solution.py:36
  125.6 3.7 %all-to-all-start.2 = ((f32[16,16,512]{2,1,0:T(8,128)}), f32[16,16,512]{2,1,0:T(8,128)S(1)}, u32[]{:S(2)}, u32[]{:S(2)}) async-start(f32[16,16,512]{2,1,0:T(8,128)} %fusion.4), calls=%async_computation.2 | async-start | bytes 1048576 | tf_op jit(solution)/shard_map/all_to_all | solution.py:36
  129.5 2.0 multiply_add_fusion
  132.0 14.0 %all-to-all-done.2 = f32[16,16,512]{2,1,0:T(8,128)S(1)} async-done(((f32[16,16,512]{2,1,0:T(8,128)}), f32[16,16,512]{2,1,0:T(8,128)S(1)}, u32[]{:S(2)}, u32[]{:S(2)}) %all-to-all-start.2) | async-done | bytes 524320 | tf_op jit(solution)/shard_map/all_to_all | solution.py:36
  146.1 14.5 %all_to_all.70 = bf16[16,16,512]{2,1,0:T(8,128)(2,1)S(1)} all-to-all(bf16[16,16,512]{2,1,0:T(8,128)(2,1)S(1)} %broadcast_in_dim.9), channel_id=1, replica_groups=mesh['grp'=2,'kv'=16,'tp'=8] {'kv'}, dimensions={0} | all-to-all | bytes 524288 | tf_op jit(solution)/shard_map/all_to_all | solution.py:13
  160.6 1.3 convolution_convert_fusion
  161.9 11.9 %all_to_all.71 = bf16[8,256,32]{1,2,0:T(8,128)(2,1)S(1)} all-to-all(bf16[8,256,32]{1,2,0:T(8,128)(2,1)S(1)} %bitcast.64), channel_id=1, replica_groups=mesh['grp'=2,'kv'=16,'tp'=8] {'tp'}, dimensions={0} | all-to-all | bytes 262144 | tf_op jit(solution)/shard_map/all_to_all | solution.py:42
  175.2 3.6 %all-to-all-start.10 = ((bf16[8,256,32]{1,2,0:T(8,128)(2,1)}), bf16[8,256,32]{1,2,0:T(8,128)(2,1)S(1)}, u32[]{:S(2)}, u32[]{:S(2)}) async-start(bf16[8,256,32]{1,2,0:T(8,128)(2,1)} %broadcast_in_dim.10), calls=%async_computation.10 | async-start | bytes 262144 | tf_op jit(solution)/shard_map/all_to_all | solution.py:13
  178.9 7.6 %all-to-all-done.10 = bf16[8,256,32]{1,2,0:T(8,128)(2,1)S(1)} async-done(((bf16[8,256,32]{1,2,0:T(8,128)(2,1)}), bf16[8,256,32]{1,2,0:T(8,128)(2,1)S(1)}, u32[]{:S(2)}, u32[]{:S(2)}) %all-to-all-start.10) | async-done | bytes 131104 | tf_op jit(solution)/shard_map/all_to_all | solution.py:13
  187.4 1.8 pad_maximum_fusion
  189.2 3.5 %copy.54 = f32[512,1408]{0,1:T(8,128)} copy(f32[512,1408]{1,0:T(8,128)} %pad_maximum_fusion) | data formatting | bytes 5767168
  192.8 12.1 %all_to_all.72 = f32[16,1,256]{2,1,0:T(1,128)S(1)} all-to-all(f32[16,1,256]{2,1,0:T(1,128)S(1)} %broadcast_in_dim.11), channel_id=1, replica_groups=mesh['grp'=2,'kv'=16,'tp'=8] {'kv'}, dimensions={0} | all-to-all | bytes 32768 | tf_op jit(solution)/shard_map/all_to_all | solution.py:13
  205.0 46.0 %reduce-scatter.4.cloned.1.call-done = f32[88,512]{1,0:T(8,128)} async-done(((f32[1408,512]{1,0:T(8,128)}), f32[88,512]{1,0:T(8,128)}) %reduce-scatter.4.cloned.1.call-update) | async-done | bytes 180240
  252.0 19.5 %all_gather.3 = bf16[256,1408]{0,1:T(8,128)(2,1)S(1)} all-gather(bf16[256,88]{0,1:T(8,128)(2,1)S(1)} %fusion.11), channel_id=1, replica_groups=mesh['grp'=2,'kv'=16,'tp'=8] {'kv'}, dimensions={1}, use_global_device_ids=true | all-gather | bytes 765952 | tf_op jit(solution)/shard_map/all_gather | solution.py:133
  271.5 1.1 convolution_convert_fusion.1
  272.5 6.4 %all-to-all-start.12 = ((bf16[8,256,32]{1,2,0:T(8,128)(2,1)}), bf16[8,256,32]{1,2,0:T(8,128)(2,1)S(1)}, u32[]{:S(2)}, u32[]{:S(2)}) async-start(bf16[8,256,32]{1,2,0:T(8,128)(2,1)} %bitcast.18), calls=%async_computation.12 | async-start | bytes 262144 | tf_op jit(solution)/shard_map/all_to_all | solution.py:42
  279.6 7.7 %all-to-all-done.12 = bf16[8,256,32]{1,2,0:T(8,128)(2,1)S(1)} async-done(((bf16[8,256,32]{1,2,0:T(8,128)(2,1)}), bf16[8,256,32]{1,2,0:T(8,128)(2,1)S(1)}, u32[]{:S(2)}, u32[]{:S(2)}) %all-to-all-start.12) | async-done | bytes 131104 | tf_op jit(solution)/shard_map/all_to_all | solution.py:42
  (83 shorter events, 15.8 us)
Async XLA Ops:
  7.2 179.4 %copy-start = (bf16[256,1408]{1,0:T(8,128)(2,1)S(1)}, bf16[256,1408]{1,0:T(8,128)(2,1)}, u32[]{:S(2)}) copy-start(bf16[256,1408]{1,0:T(8,128)(2,1)} %param.30) | copy-start | bytes 2162692
  7.2 39.2 %copy-start.8 = (bf16[256,32]{0,1:T(8,128)(2,1)S(1)}, bf16[256,32]{0,1:T(8,128)(2,1)}, u32[]{:S(2)}) copy-start(bf16[256,32]{0,1:T(8,128)(2,1)} %param.22) | copy-start | bytes 49156
  8.7 15.8 %all-to-all-start = ((bf16[8,256,32]{1,2,0:T(8,128)(2,1)}), bf16[8,256,32]{1,2,0:T(8,128)(2,1)S(1)}, u32[]{:S(2)}, u32[]{:S(2)}) async-start(bf16[8,256,32]{1,2,0:T(8,128)(2,1)} %broadcast_in_dim.8), calls=%async_computation | async-start | bytes 262144 | tf_op jit(solution)/shard_map/all_to_all | solution.py:13
  16.5 40.1 %copy-start.9 = (bf16[256,32]{0,1:T(8,128)(2,1)S(1)}, bf16[256,32]{0,1:T(8,128)(2,1)}, u32[]{:S(2)}) copy-start(bf16[256,32]{0,1:T(8,128)(2,1)} %param.23) | copy-start | bytes 49156
  25.2 27.4 %all-to-all-start.1 = ((f32[16,1,16]{2,1,0:T(1,128)}), f32[16,1,16]{2,1,0:T(1,128)S(1)}, u32[]{:S(2)}, u32[]{:S(2)}) async-start(f32[16,1,16]{2,1,0:T(1,128)} %all_to_all.44), calls=%async_computation.1 | async-start | bytes 16384 | tf_op jit(solution)/shard_map/all_to_all | solution.py:36
  45.5 22.4 %copy-start.5 = (bf16[256,256]{1,0:T(8,128)(2,1)S(1)}, bf16[256,256]{1,0:T(8,128)(2,1)}, u32[]{:S(2)}) copy-start(bf16[256,256]{1,0:T(8,128)(2,1)} %param.19) | copy-start | bytes 393220
  46.0 33.3 %copy-start.10 = (f32[16,4]{0,1:T(4,128)S(1)}, f32[16,4]{0,1:T(4,128)}, u32[]{:S(2)}) copy-start(f32[16,4]{0,1:T(4,128)} %param.26) | copy-start | bytes 772
  46.0 33.4 %copy-start.6 = (bf16[256,256]{1,0:T(8,128)(2,1)S(1)}, bf16[256,256]{1,0:T(8,128)(2,1)}, u32[]{:S(2)}) copy-start(bf16[256,256]{1,0:T(8,128)(2,1)} %param.18) | copy-start | bytes 393220
  46.0 49.0 %copy-start.3 = (bf16[256,512]{1,0:T(8,128)(2,1)S(1)}, bf16[256,512]{1,0:T(8,128)(2,1)}, u32[]{:S(2)}) copy-start(bf16[256,512]{1,0:T(8,128)(2,1)} %param.20) | copy-start | bytes 786436
  46.4 49.6 %copy-start.4 = (bf16[256,512]{1,0:T(8,128)(2,1)S(1)}, bf16[256,512]{1,0:T(8,128)(2,1)}, u32[]{:S(2)}) copy-start(bf16[256,512]{1,0:T(8,128)(2,1)} %param.21) | copy-start | bytes 786436
  52.6 11.6 %all-to-all-start.5 = ((f32[16,1,512]{2,1,0:T(1,128)}), f32[16,1,512]{2,1,0:T(1,128)S(1)}, u32[]{:S(2)}, u32[]{:S(2)}) async-start(f32[16,1,512]{2,1,0:T(1,128)} %reshape.179), calls=%async_computation.5 | async-start | bytes 65536 | tf_op jit(solution)/shard_map/all_to_all | solution.py:36
  64.2 11.3 %all-to-all-start.4 = ((f32[16,1,512]{2,1,0:T(1,128)}), f32[16,1,512]{2,1,0:T(1,128)S(1)}, u32[]{:S(2)}, u32[]{:S(2)}) async-start(f32[16,1,512]{2,1,0:T(1,128)} %reshape.181), calls=%async_computation.4 | async-start | bytes 65536 | tf_op jit(solution)/shard_map/all_to_all | solution.py:36
  75.5 15.7 %all-to-all-start.6 = ((f32[16,16,256]{2,1,0:T(8,128)}), f32[16,16,256]{2,1,0:T(8,128)S(1)}, u32[]{:S(2)}, u32[]{:S(2)}) async-start(f32[16,16,256]{2,1,0:T(8,128)} %fusion.6), calls=%async_computation.6 | async-start | bytes 524288 | tf_op jit(solution)/shard_map/all_to_all | solution.py:36
  91.2 14.4 %all-to-all-start.3 = ((f32[16,16,256]{2,1,0:T(8,128)}), f32[16,16,256]{2,1,0:T(8,128)S(1)}, u32[]{:S(2)}, u32[]{:S(2)}) async-start(f32[16,16,256]{2,1,0:T(8,128)} %fusion.8), calls=%async_computation.3 | async-start | bytes 524288 | tf_op jit(solution)/shard_map/all_to_all | solution.py:36
  95.0 17.0 %copy-start.7 = (f32[16,4,64]{2,1,0:T(4,128)S(1)}, f32[16,4,64]{2,1,0:T(4,128)}, u32[]{:S(2)}) copy-start(f32[16,4,64]{2,1,0:T(4,128)} %param.25) | copy-start | bytes 49156
  105.6 20.0 %all-to-all-start.7 = ((f32[16,16,512]{2,1,0:T(8,128)}), f32[16,16,512]{2,1,0:T(8,128)S(1)}, u32[]{:S(2)}, u32[]{:S(2)}) async-start(f32[16,16,512]{2,1,0:T(8,128)} %fusion.2), calls=%async_computation.7 | async-start | bytes 1048576 | tf_op jit(solution)/shard_map/all_to_all | solution.py:36
  125.6 20.4 %all-to-all-start.2 = ((f32[16,16,512]{2,1,0:T(8,128)}), f32[16,16,512]{2,1,0:T(8,128)S(1)}, u32[]{:S(2)}, u32[]{:S(2)}) async-start(f32[16,16,512]{2,1,0:T(8,128)} %fusion.4), calls=%async_computation.2 | async-start | bytes 1048576 | tf_op jit(solution)/shard_map/all_to_all | solution.py:36
  131.5 30.4 %copy-start.1 = (f32[16,4,64,128]{3,2,1,0:T(8,128)}, f32[16,4,64,128]{3,2,1,0:T(8,128)S(1)}, u32[]{:S(2)}) copy-start(f32[16,4,64,128]{3,2,1,0:T(8,128)S(1)} %multiply_add_fusion) | copy-start | bytes 6291460
  131.5 47.4 %copy-start.12 = (bf16[256]{0:T(256)(128)(2,1)S(1)}, bf16[256]{0:T(256)(128)(2,1)}, u32[]{:S(2)}) copy-start(bf16[256]{0:T(256)(128)(2,1)} %param.28) | copy-start | bytes 1540
  160.6 26.4 %copy-start.2 = (bf16[256,1408]{1,0:T(8,128)(2,1)S(1)}, bf16[256,1408]{1,0:T(8,128)(2,1)}, u32[]{:S(2)}) copy-start(bf16[256,1408]{1,0:T(8,128)(2,1)} %param.29) | copy-start | bytes 2162692
  175.2 11.2 %all-to-all-start.10 = ((bf16[8,256,32]{1,2,0:T(8,128)(2,1)}), bf16[8,256,32]{1,2,0:T(8,128)(2,1)S(1)}, u32[]{:S(2)}, u32[]{:S(2)}) async-start(bf16[8,256,32]{1,2,0:T(8,128)(2,1)} %broadcast_in_dim.10), calls=%async_computation.10 | async-start | bytes 262144 | tf_op jit(solution)/shard_map/all_to_all | solution.py:13
  178.8 72.2 %reduce-scatter.4.cloned.1.call-start = ((), (), s32[]{:S(2)}) async-start(), calls=%async_computation.14 | async-start | bytes 3063808
  192.7 78.8 %copy-start.11 = (bf16[1408,256]{1,0:T(8,128)(2,1)S(1)}, bf16[1408,256]{1,0:T(8,128)(2,1)}, u32[]{:S(2)}) copy-start(bf16[1408,256]{1,0:T(8,128)(2,1)} %param.31) | copy-start | bytes 2162692
  272.5 14.8 %all-to-all-start.12 = ((bf16[8,256,32]{1,2,0:T(8,128)(2,1)}), bf16[8,256,32]{1,2,0:T(8,128)(2,1)S(1)}, u32[]{:S(2)}, u32[]{:S(2)}) async-start(bf16[8,256,32]{1,2,0:T(8,128)(2,1)} %bitcast.18), calls=%async_computation.12 | async-start | bytes 262144 | tf_op jit(solution)/shard_map/all_to_all | solution.py:42
Sparse Core Ops, SparseCore 0:
  192.9 58.0 reduce-scatter.3
where the time goes:
time: 296 us; the launch traced here: 295 us
  waiting for transfers between devices  134 us (45%)
  starting transfers between devices  60.8 us (21%)
  blocking collectives  58 us (20%)
  between operations  14.4 us (5%)
  local copies, waits for them, and re-layouts  10.2 us (3%)
  other arithmetic  9.97 us (3%)
  matrix products  7.66 us (3%)
    all_to_all x7, waiting for transfers between devices, summed_on_arrival(): pieces = lax.all_to_all(split_up(array, dim, count), axis, 0, 0, tiled=True)  65.2 us
    unnamed x2, waiting for transfers between devices  46 us
    all_to_all x7, starting transfers between devices, summed_on_arrival(): pieces = lax.all_to_all(split_up(array, dim, count), axis, 0, 0, tiled=True)  42.9 us
    all_to_all x2, blocking collectives, copy_for_each(): lax.all_to_all(jnp.broadcast_to(array[None], (count, *array.shape)), axis...  26.6 us
    all_gather x1, blocking collectives, shards(): lax.all_gather(hidden_share, 'kv', axis=1, tiled=True)  19.5 us
    all_to_all x2, waiting for transfers between devices, copy_for_each(): lax.all_to_all(jnp.broadcast_to(array[None], (count, *array.shape)), axis...  14.8 us
    all_to_all x1, blocking collectives, sum_at_owner(): pieces = lax.all_to_all(split_up(array, dim, count), axis, 0, 0, tiled=True)  11.9 us
    all_to_all x2, starting transfers between devices, copy_for_each(): lax.all_to_all(jnp.broadcast_to(array[None], (count, *array.shape)), axis...  11.4 us
  transfers between devices with their start and end apart: 11, of which 11 were waited for; matrix products, arithmetic and copies ran while one was open for 5% of the time, Pallas kernels for 0%

commit v1 on v0

v1 whole, which is shorter than its diff:
```python
import functools

import jax
import jax.numpy as jnp
from jax import lax
from jax.experimental import pallas as pl
from jax.experimental.pallas import tpu as pltpu
from jax.sharding import PartitionSpec as P

DQK = 64
DV = 128
LANES = 128
HALF = LANES // 2
F32 = jnp.float32
BF16 = jnp.bfloat16
MESH = pl.DeviceIdType.MESH


def far_first(count):
    return sorted(range(1, count), key=lambda d: -min(d, count - d))


def near_first(count):
    return far_first(count)[::-1]


def column_pieces(width, step=256):
    return [(at, min(step, width - at)) for at in range(0, width, step)]


def hi_lo(values, lane):
    high = values.astype(BF16).astype(F32)
    return jnp.where(lane < HALF, high, values - high).astype(BF16)


def from_hi_lo(tile):
    return tile[:, :HALF] + tile[:, HALF:]


def layer_kernel(
    n_kv, n_tp,
    tokens_h, norm_gain, wq_h, wk_h, wv_h, wo_h, wi_h, wf_h, mem_h, norm_h, stab_h, wmix_h, ffn_gain, wg_h, wu_h, wd_h,
    out_ref, newmem_h, newnorm_ref, newstab_ref,
    tokens, w1, wgates, mem, norm, stab, wmix, wmix_t, w2, wd, wd_t,
    token_t, x_raw, z1_pair, z1_own, z1_got, z1_send, z1_recv,
    numer, gated, mix_send, mix_recv, mixed_t, z2_pair, z2_own, z2_got, z2_send, z2_recv, hidden, down_send, down_recv,
    local_sem, tok_s, tok_r, p1_s, p1_r, a_s, a_r, g_s, g_r, gf_s, gf_r, m_s, m_r, x_s, x_r, p2_s, p2_r, b_s, b_r, h_s, h_r, hf_s, hf_r, d_s, d_r,
):
    kv, tp = lax.axis_index("kv"), lax.axis_index("tp")
    n_y = n_kv // 2
    core, y = lax.rem(kv, 2), kv // 2
    other = 1 - core
    partner = 2 * y + other
    own = mem.shape[0]
    heads = mem.shape[1]
    feats = token_t.shape[0]
    mine = tokens.shape[1]
    half_rows = n_y * own
    n_feats = feats * n_kv

    def y_of(d):
        return lax.rem(y + d, n_y)

    def from_y(d):
        return lax.rem(y + n_y - d, n_y)

    def tp_of(d):
        return lax.rem(tp + d, n_tp)

    def from_tp(d):
        return lax.rem(tp + n_tp - d, n_tp)

    def rows(index, size):
        return pl.ds(pl.multiple_of(index * size, size), size)

    barrier = pltpu.get_barrier_semaphore()
    for d in far_first(n_tp):
        pl.semaphore_signal(barrier, inc=1, device_id={"tp": tp_of(d)}, device_id_type=MESH)
    for d in far_first(n_y):
        pl.semaphore_signal(barrier, inc=1, device_id={"kv": 2 * y_of(d) + core}, device_id_type=MESH)
    pl.semaphore_signal(barrier, inc=1, device_id={"kv": partner}, device_id_type=MESH)

    dq, dk, dv = wq_h.shape[1], wk_h.shape[1], wv_h.shape[1]
    n_main = dq + dk + 2 * dv
    n_ff = wg_h.shape[1]
    n_gate = wi_h.shape[1]
    loads = {}
    for i, (name, source, target) in enumerate((
        ("tokens", tokens_h, tokens),
        ("wi", wi_h, wgates.at[0]),
        ("wf", wf_h, wgates.at[1]),
        ("wq", wq_h, w1.at[:, pl.ds(0, dq)]),
        ("wk", wk_h, w1.at[:, pl.ds(dq, dk)]),
        ("wv", wv_h, w1.at[:, pl.ds(dq + dk, dv)]),
        ("wo", wo_h, w1.at[:, pl.ds(dq + dk + dv, dv)]),
        ("mix", wmix_h, wmix),
        ("down", wd_h, wd),
        ("mem", mem_h, mem),
        ("norm", norm_h, norm),
        ("stab", stab_h, stab),
        ("gate", wg_h, w2.at[:, pl.ds(0, n_ff)]),
        ("up", wu_h, w2.at[:, pl.ds(n_ff, n_ff)]),
    )):
        loads[name] = pltpu.make_async_copy(source, target, local_sem.at[i])
        loads[name].start()
    sent = []

    def send(source, target, send_sem, recv_sem, where):
        copy = pltpu.make_async_remote_copy(
            src_ref=source, dst_ref=target, send_sem=send_sem, recv_sem=recv_sem, device_id=where, device_id_type=MESH
        )
        copy.start()
        sent.append(copy)

    def arrive(target, send_sem, recv_sem, where):
        pltpu.make_async_remote_copy(
            src_ref=target, dst_ref=target, send_sem=send_sem, recv_sem=recv_sem, device_id=where, device_id_type=MESH
        ).wait_recv()

    loads["tokens"].wait()
    token_t[rows(tp, mine), :] = tokens[...].astype(F32).T.astype(BF16)
    pl.semaphore_wait(barrier, (n_tp - 1) + (n_y - 1) + 1)
    for d in far_first(n_tp):
        part = token_t.at[rows(tp, mine), :]
        send(part, part, tok_s.at[d], tok_r.at[d], {"tp": tp_of(d)})

    loads["wi"].wait()
    loads["wf"].wait()
    lane_w = lax.broadcasted_iota(jnp.int32, (n_gate, LANES), 1)
    row_w = lax.broadcasted_iota(jnp.int32, (n_gate, LANES), 0)
    low_lane = lax.rem(lane_w, HALF)
    head_row = row_w - tp * heads
    pick_i = jnp.where((low_lane == head_row) & (head_row < heads) & (head_row >= 0), 1.0, 0.0).astype(BF16)
    pick_f = jnp.where((low_lane == head_row + heads) & (head_row < heads) & (head_row >= 0), 1.0, 0.0).astype(BF16)
    w1[:, n_main:] = (
        jnp.dot(wgates[0], pick_i, preferred_element_type=F32) + jnp.dot(wgates[1], pick_f, preferred_element_type=F32)
    ).astype(BF16)

    loads["mix"].wait()
    wmix_t[...] = wmix[...].T
    loads["down"].wait()
    for at, width in column_pieces(wd.shape[0]):
        wd_t[:, at : at + width] = wd[at : at + width, :].T
    for name in ("wq", "wk", "wv", "wo"):
        loads[name].wait()

    for d in near_first(n_tp):
        arrive(token_t.at[rows(from_tp(d), mine), :], tok_s.at[d], tok_r.at[d], {"tp": tp_of(d)})

    lane = lax.broadcasted_iota(jnp.int32, (half_rows, LANES), 1)

    def project(gain, weights, widths, square_lane, gates, core_of, store):
        wide = x_raw[:, core_of].reshape(half_rows, feats).astype(F32)
        normed = (wide * gain[...].astype(F32)).astype(BF16)
        squares = jnp.sum(wide * wide, axis=1, keepdims=True)
        for at, width in widths:
            store(at, width, jnp.dot(normed, weights[:, at : at + width], preferred_element_type=F32))
        end = widths[-1][0] + widths[-1][1]
        tile = jnp.broadcast_to(squares, (half_rows, LANES))
        if gates:
            last = jnp.dot(normed, weights[:, end : end + LANES], preferred_element_type=F32)
            tile = jnp.where(lax.rem(lane, HALF) == square_lane, tile, last)
        store(end, LANES, tile)

    def reduce_over_kv(gain, weights, width, square_lane, gates, pair, own_z, got, out, into, sems, total_at):
        p_s, p_r, r_s, r_r = sems
        pieces = column_pieces(width)

        def to_partner(at, size, z):
            value = hi_lo(z, lane) if at == width else z.astype(BF16)
            pair[:, :, at : at + size] = value.reshape(n_y, own, size)

        def keep(at, size, z):
            own_z[:, :, at : at + size] = z.reshape(n_y, own, size)

        project(gain, weights, pieces, square_lane, gates, other, to_partner)
        send(pair, got, p_s, p_r, {"kv": partner})
        project(gain, weights, pieces, square_lane, gates, core, keep)
        arrive(got, p_s, p_r, {"kv": partner})
        small_lane = lax.broadcasted_iota(jnp.int32, (own, LANES), 1)
        for d in far_first(n_y) + [0]:
            at_y = y_of(d)
            for at, size in pieces + [(width, LANES)]:
                both = own_z[at_y, :, at : at + size]
                other_half = got[at_y, :, at : at + size].astype(F32)
                if at == width:
                    both = both + (other_half + jnp.concatenate([other_half[:, HALF:], other_half[:, :HALF]], axis=1))
                    if d:
                        both = hi_lo(both, small_lane)
                else:
                    both = both + other_half
                if d:
                    out[d, :, at : at + size] = both.astype(BF16)
                else:
                    total_at[:, at : at + size] = both
            if d:
                send(out.at[d], into.at[d], r_s.at[d], r_r.at[d], {"kv": 2 * at_y + core})
        for d in near_first(n_y):
            arrive(into.at[d], r_s.at[d], r_r.at[d], {"kv": 2 * y_of(d) + core})

    def total_of(total_at, into, at, size):
        value = total_at[:, at : at + size]
        for d in range(1, n_y):
            value = value + into[d, :, at : at + size].astype(F32)
        return value

    def tile_of(total_at, into, at):
        rest = into[1, :, at : at + LANES].astype(F32)
        for d in range(2, n_y):
            rest = rest + into[d, :, at : at + LANES].astype(F32)
        return total_at[:, at : at + HALF] + from_hi_lo(rest)

    def gather_over_kv(buffer, sems):
        r_s, r_r, f_s, f_r = sems
        part = buffer.at[rows(kv, own), :]
        for d in far_first(n_y):
            send(part, part, r_s.at[d], r_r.at[d], {"kv": 2 * y_of(d) + core})
        send(part, part, f_s.at[0], f_r.at[0], {"kv": partner})

        def finish():
            for d in near_first(n_y):
                got = buffer.at[rows(2 * from_y(d) + core, own), :]
                arrive(got, r_s.at[d], r_r.at[d], {"kv": 2 * y_of(d) + core})
                send(got, got, f_s.at[d], f_r.at[d], {"kv": partner})
            for d in [0] + near_first(n_y):
                arrive(buffer.at[rows(2 * from_y(d) + other, own), :], f_s.at[d], f_r.at[d], {"kv": partner})

        return finish

    def sum_over_tp(partial, out, into, sems):
        s, r = sems
        out[...] = partial.astype(BF16).reshape(n_tp, mine, partial.shape[1])
        for d in far_first(n_tp):
            send(out.at[tp_of(d)], into.at[d], s.at[d], r.at[d], {"tp": tp_of(d)})
        total = out[tp].astype(F32)
        for d in near_first(n_tp):
            arrive(into.at[d], s.at[d], r.at[d], {"tp": tp_of(d)})
            total = total + into[d].astype(F32)
        return total

    z_total = z1_own.at[y]
    x_raw[...] = token_t[...].T.reshape(x_raw.shape)
    reduce_over_kv(
        norm_gain, w1, n_main, 2 * heads, True, z1_pair, z1_own, z1_got, z1_send, z1_recv, (p1_s, p1_r, a_s, a_r), z_total
    )
    gates = tile_of(z_total, z1_recv, n_main)
    scale1 = lax.rsqrt(gates[:, 2 * heads : 2 * heads + 1] / n_feats + 1e-06)
    query = scale1 * total_of(z_total, z1_recv, 0, dq) * DQK ** (-0.5)
    key = scale1 * total_of(z_total, z1_recv, dq, dk)
    value = scale1 * total_of(z_total, z1_recv, dq + dk, dv)
    outgate = scale1 * total_of(z_total, z1_recv, dq + dk + dv, dv)
    igate = scale1 * gates[:, :heads]
    forget = scale1 * gates[:, heads : 2 * heads]
    lforget = jnp.minimum(forget, 0.0) - jnp.log1p(jnp.exp(-jnp.abs(forget)))
    loads["stab"].wait()
    loads["norm"].wait()
    loads["mem"].wait()
    held = lforget + stab[...]
    new_stab = jnp.maximum(held, igate)
    newstab_ref[...] = new_stab
    decay = jnp.exp(held - new_stab)
    inflow = jnp.exp(igate - new_stab)
    floor = jnp.exp(-new_stab)
    query_t = query.T
    for s in range(own):
        for h in range(heads):
            column = query_t[h * DQK : (h + 1) * DQK, s : s + 1]
            numer[s : s + 1, h * DV : (h + 1) * DV] = jnp.sum(column * mem[s, h], axis=0, keepdims=True)
    for h in range(heads):
        q, k = query[:, h * DQK : (h + 1) * DQK], key[:, h * DQK : (h + 1) * DQK]
        keep, add = decay[:, h : h + 1], inflow[:, h : h + 1]
        new_norm = keep * norm[:, h, :] + add * k
        newnorm_ref[:, h, :] = new_norm
        denom = jnp.maximum(jnp.abs(jnp.sum(q * new_norm, axis=1, keepdims=True)), floor[:, h : h + 1])
        at = slice(h * DV, (h + 1) * DV)
        top = keep * numer[:, at] + (add * jnp.sum(q * k, axis=1, keepdims=True)) * value[:, at]
        gated[rows(kv, own), at] = (jax.nn.sigmoid(outgate[:, at]) * (top / denom)).astype(BF16)
    finish = gather_over_kv(gated, (g_s, g_r, gf_s, gf_r))

    spread = jnp.concatenate([jnp.broadcast_to(inflow[:, h : h + 1], (own, DQK)) for h in range(heads)], axis=1)
    key_t = (key * spread).T
    for s in range(own):
        for h in range(heads):
            column = key_t[h * DQK : (h + 1) * DQK, s : s + 1]
            mem[s, h] = decay[s : s + 1, h : h + 1] * mem[s, h] + column * value[s : s + 1, h * DV : (h + 1) * DV]
    put = pltpu.make_async_copy(mem, newmem_h, local_sem.at[14])
    put.start()
    finish()

    partial = lax.dot_general(wmix_t[...], gated[...], (((1,), (1,)), ((), ())), preferred_element_type=F32)
    total = sum_over_tp(partial, mix_send, mix_recv, (m_s, m_r))
    mixed = (token_t[rows(tp, mine), :].astype(F32) + total).astype(BF16)
    mixed_t[rows(tp, mine), :] = mixed
    for d in far_first(n_tp):
        part = mixed_t.at[rows(tp, mine), :]
        send(part, part, x_s.at[d], x_r.at[d], {"tp": tp_of(d)})
    loads["gate"].wait()
    loads["up"].wait()
    for d in near_first(n_tp):
        arrive(mixed_t.at[rows(from_tp(d), mine), :], x_s.at[d], x_r.at[d], {"tp": tp_of(d)})

    u_total = z2_own.at[y]
    x_raw[...] = mixed_t[...].T.reshape(x_raw.shape)
    reduce_over_kv(
        ffn_gain, w2, 2 * n_ff, 0, False, z2_pair, z2_own, z2_got, z2_send, z2_recv, (p2_s, p2_r, b_s, b_r), u_total
    )
    squares = tile_of(u_total, z2_recv, 2 * n_ff)[:, :1]
    scale2 = lax.rsqrt(squares / n_feats + 1e-06)
    for at, size in column_pieces(n_ff):
        gate = scale2 * total_of(u_total, z2_recv, at, size)
        up = scale2 * total_of(u_total, z2_recv, n_ff + at, size)
        hidden[rows(kv, own), at : at + size] = (gate * jax.nn.sigmoid(gate) * up).astype(BF16)
    gather_over_kv(hidden, (h_s, h_r, hf_s, hf_r))()

    partial = lax.dot_general(wd_t[...], hidden[...], (((1,), (1,)), ((), ())), preferred_element_type=F32)
    total = sum_over_tp(partial, down_send, down_recv, (d_s, d_r))
    out_ref[...] = (mixed_t[rows(tp, mine), :].astype(F32) + total).astype(BF16)
    put.wait()
    for copy in sent:
        copy.wait_send()


def shards(n_kv, n_tp, tokens, norm_gain, w_query, w_key, w_value, w_outgate, w_input_gate, w_forget_gate, memory, normalizer, stabilizer, w_mix_out, ffn_gain, w_gate, w_up, w_down):
    seqs, mine = tokens.shape
    feats = norm_gain.shape[0]
    n_y = n_kv // 2
    own = memory.shape[0]
    dv = w_value.shape[1]
    n1 = w_query.shape[1] + w_key.shape[1] + 2 * dv + LANES
    n_ff = w_gate.shape[1]
    n2 = 2 * n_ff + LANES
    out_feats = w_mix_out.shape[1]
    hbm = pl.BlockSpec(memory_space=pltpu.HBM)
    vmem = pl.BlockSpec(memory_space=pltpu.VMEM)
    dma = pltpu.SemaphoreType.DMA
    ys, xs, one = dma((n_y,)), dma((n_tp,)), dma
    out_t, new_memory, new_normalizer, new_stabilizer = pl.pallas_call(
        functools.partial(layer_kernel, n_kv, n_tp),
        out_shape=(
            jax.ShapeDtypeStruct((mine, seqs), BF16),
            jax.ShapeDtypeStruct(memory.shape, F32),
            jax.ShapeDtypeStruct(normalizer.shape, F32),
            jax.ShapeDtypeStruct(stabilizer.shape, F32),
        ),
        in_specs=[hbm, vmem] + [hbm] * 10 + [vmem] + [hbm] * 3,
        out_specs=(vmem, hbm, vmem, vmem),
        scratch_shapes=[
            pltpu.VMEM(tokens.shape, BF16),
            pltpu.VMEM((feats, n1), BF16),
            pltpu.VMEM((2, *w_input_gate.shape), BF16),
            pltpu.VMEM(memory.shape, F32),
            pltpu.VMEM(normalizer.shape, F32),
            pltpu.VMEM(stabilizer.shape, F32),
            pltpu.VMEM(w_mix_out.shape, BF16),
            pltpu.VMEM(w_mix_out.shape[::-1], BF16),
            pltpu.VMEM((feats, 2 * n_ff), BF16),
            pltpu.VMEM(w_down.shape, BF16),
            pltpu.VMEM(w_down.shape[::-1], BF16),
            pltpu.VMEM((feats, seqs), BF16),
            pltpu.VMEM((n_y, 2, own, feats), BF16),
            pltpu.VMEM((n_y, own, n1), BF16),
            pltpu.VMEM((n_y, own, n1), F32),
            pltpu.VMEM((n_y, own, n1), BF16),
            pltpu.VMEM((n_y, own, n1), BF16),
            pltpu.VMEM((n_y, own, n1), BF16),
            pltpu.VMEM((own, dv), F32),
            pltpu.VMEM((seqs, dv), BF16),
            pltpu.VMEM((n_tp, mine, seqs), BF16),
            pltpu.VMEM((n_tp, mine, seqs), BF16),
            pltpu.VMEM((out_feats, seqs), BF16),
            pltpu.VMEM((n_y, own, n2), BF16),
            pltpu.VMEM((n_y, own, n2), F32),
            pltpu.VMEM((n_y, own, n2), BF16),
            pltpu.VMEM((n_y, own, n2), BF16),
            pltpu.VMEM((n_y, own, n2), BF16),
            pltpu.VMEM((seqs, n_ff), BF16),
            pltpu.VMEM((n_tp, mine, seqs), BF16),
            pltpu.VMEM((n_tp, mine, seqs), BF16),
            dma((15,)),
            xs, xs,
            one, one, ys, ys,
            ys, ys, ys, ys,
            xs, xs,
            xs, xs,
            one, one, ys, ys,
            ys, ys, ys, ys,
            xs, xs,
        ],
        compiler_params=pltpu.CompilerParams(collective_id=0, has_side_effects=True, vmem_limit_bytes=48 * 1024 * 1024),
        name="layer",
    )(
        tokens, norm_gain.reshape(1, -1), w_query, w_key, w_value, w_outgate, w_input_gate, w_forget_gate,
        memory, normalizer, stabilizer, w_mix_out, ffn_gain.reshape(1, -1), w_gate, w_up, w_down,
    )
    return out_t.T, new_memory, new_normalizer, new_stabilizer


def solution(mesh):
    in_specs = (
        P("grp", ("kv", "tp")),
        P("kv"),
        P("kv", "tp"),
        P("kv", "tp"),
        P("kv", "tp"),
        P("kv", "tp"),
        P("kv", None),
        P("kv", None),
        P(("grp", "kv"), "tp", None, None),
        P(("grp", "kv"), "tp", None),
        P(("grp", "kv"), "tp"),
        P("tp", "kv"),
        P("kv"),
        P("kv", "tp"),
        P("kv", "tp"),
        P("tp", "kv"),
    )
    out_specs = (
        P("grp", ("kv", "tp")),
        P(("grp", "kv"), "tp", None, None),
        P(("grp", "kv"), "tp", None),
        P(("grp", "kv"), "tp"),
    )
    body = functools.partial(shards, mesh.shape["kv"], mesh.shape["tp"])
    return jax.shard_map(body, mesh=mesh, in_specs=in_specs, out_specs=out_specs, check_vma=False)
```

time: 296 us -> 116 us (0.39)
  waiting for transfers between devices: 134 us -> 0 us
  Pallas kernels: 0 us -> 98.7 us
  starting transfers between devices: 60.8 us -> 0 us
  blocking collectives: 58 us -> 0 us
  between operations: 14.4 us -> 0.66 us
  other arithmetic: 9.97 us -> 0 us
  matrix products: 7.66 us -> 0 us
  local copies, waits for them, and re-layouts: 10.2 us -> 16.5 us
    pallas_call x0 -> x1, Pallas kernels: none -> 98.7 us  [shards(): pl.pallas_call(functools.partial(layer_kernel, n_kv, n_tp), out_shape=(ja...]
    all_to_all x10 -> x0, waiting for transfers between devices: 87.7 us -> none  [the longest x7 65.2 us: summed_on_arrival(): pieces = lax.all_to_all(split_up(array, dim, count), axis, 0, 0, tiled=True)]
    all_to_all x10 -> x0, starting transfers between devices: 60.7 us -> none  [the longest x7 42.9 us: summed_on_arrival(): pieces = lax.all_to_all(split_up(array, dim, count), axis, 0, 0, tiled=True)]
    unnamed x2 -> x0, waiting for transfers between devices: 46 us -> none
    all_to_all x3 -> x0, blocking collectives: 38.5 us -> none  [the longest x2 26.6 us: copy_for_each(): lax.all_to_all(jnp.broadcast_to(array[None], (count, *array.shape)), axis...]
    all_gather x1 -> x0, blocking collectives: 19.5 us -> none  [shards(): lax.all_gather(hidden_share, 'kv', axis=1, tiled=True)]
    unnamed x33 -> x26, local copies, waits for them, and re-layouts: 5.94 us -> 15.2 us
    dot_general x11 -> x0, matrix products: 7.66 us -> none  [the longest x6 4.12 us: shards(): jnp.dot(normed, weight, preferred_element_type=jnp.float32)]
  transfers between devices with their start and end apart: 11 -> 0, of which waited for: 11 -> 0; matrix products, arithmetic and copies ran while one was open for 5% -> 0% of each run, Pallas kernels for 0% -> 0%
where the time goes in v1:
time: 116 us
  Pallas kernels  98.7 us (85%)
  local copies, waits for them, and re-layouts  16.5 us (14%)
    pallas_call x1, Pallas kernels, shards(): pl.pallas_call(functools.partial(layer_kernel, n_kv, n_tp), out_shape=(ja...  98.7 us
    unnamed x26, local copies, waits for them, and re-layouts  15.2 us

profile of v1, /device:TPU:513, one launch (start us, length us, event | category | flops | bytes accessed | tf_op | source)
XLA Modules:
  0.0 115.9 jit_solution(3522205928140121823)
XLA Ops:
  0.6 0.7 reshape.14.norm_gain
  1.3 0.7 reshape.15.ffn_gain
  1.9 0.8 copy.23.stab_h
  2.7 0.8 copy.20.tokens_h
  3.5 0.8 copy.21.wi_h
  4.4 0.8 copy.22.wf_h
  5.2 0.0 copy-start
  5.2 1.1 copy-done
  6.3 0.0 copy-start.1
  6.3 1.1 copy-done.1
  7.4 0.0 copy-start.2
  7.4 1.1 copy-done.2
  8.6 0.0 copy-start.3
  8.6 0.9 copy-done.3
  9.5 0.0 copy-start.4
  9.5 0.9 copy-done.4
  10.5 0.0 copy-start.5
  10.5 0.9 copy-done.5
  11.4 0.0 copy-start.6
  11.4 0.9 copy-done.6
  12.3 0.0 copy-start.7
  12.3 0.9 copy-done.7
  13.2 0.0 copy-start.8
  13.2 0.8 copy-done.8
  14.0 98.7 %layer.1 = (bf16[32,256]{1,0:T(8,128)(2,1)S(1)}, f32[16,4,64,128]{3,2,1,0:T(8,128)S(1)}, f32[16,4,64]{2,1,0:T(4,128)S(1)}, f32[16,4]{1,0:T(8,128)S(1)}) custom-call(bf16[256,32]{1,0:T(8,128)(2,1)S(1)} %copy.20.tokens_h, bf16[1,256]{1,0:T(2,128)(2,1)S(1)} %reshape.14.norm_gain, bf16[256,256]{1,0:T(8,128)(2,1)S(1)} %copy-done.6, ...), custom_call_target="tpu_custom_call" | custom-call | tf_op jit(solution)/shard_map/layer/pallas_call | solution.py:337
  112.7 0.7 copy.24
  113.3 0.6 copy.28
  113.9 1.3 %copy.29 = f32[16,4,64,128]{3,2,1,0:T(8,128)} copy(f32[16,4,64,128]{3,2,1,0:T(8,128)S(1)} %get-tuple-element.21) | data formatting | bytes 4194304
  115.2 0.6 copy.30
Async XLA Ops:
  5.2 1.1 copy-start
  6.3 1.1 copy-start.1
  7.4 1.1 copy-start.2
  8.6 0.9 copy-start.3
  9.5 0.9 copy-start.4
  10.5 0.9 copy-start.5
  11.4 0.9 copy-start.6
  12.3 0.9 copy-start.7
  13.2 0.8 copy-start.8

commit v2 on v1

--- a/solution.py
+++ b/solution.py
@@ -41,7 +41,7 @@
     n_kv, n_tp,
     tokens_h, norm_gain, wq_h, wk_h, wv_h, wo_h, wi_h, wf_h, mem_h, norm_h, stab_h, wmix_h, ffn_gain, wg_h, wu_h, wd_h,
     out_ref, newmem_h, newnorm_ref, newstab_ref,
-    tokens, w1, wgates, mem, norm, stab, wmix, wmix_t, w2, wd, wd_t,
+    w1, wgates, mem, norm, stab, wmix, wmix_t, w2, wd, wd_t,
     token_t, x_raw, z1_pair, z1_own, z1_got, z1_send, z1_recv,
     numer, gated, mix_send, mix_recv, mixed_t, z2_pair, z2_own, z2_got, z2_send, z2_recv, hidden, down_send, down_recv,
     local_sem, tok_s, tok_r, p1_s, p1_r, a_s, a_r, g_s, g_r, gf_s, gf_r, m_s, m_r, x_s, x_r, p2_s, p2_r, b_s, b_r, h_s, h_r, hf_s, hf_r, d_s, d_r,
@@ -54,7 +54,7 @@
     own = mem.shape[0]
     heads = mem.shape[1]
     feats = token_t.shape[0]
-    mine = tokens.shape[1]
+    mine = tokens_h.shape[0]
     half_rows = n_y * own
     n_feats = feats * n_kv
 
@@ -83,12 +83,12 @@
     dq, dk, dv = wq_h.shape[1], wk_h.shape[1], wv_h.shape[1]
     n_main = dq + dk + 2 * dv
     n_ff = wg_h.shape[1]
-    n_gate = wi_h.shape[1]
+    n_gate = wi_h.shape[0]
     loads = {}
     for i, (name, source, target) in enumerate((
-        ("tokens", tokens_h, tokens),
-        ("wi", wi_h, wgates.at[0]),
-        ("wf", wf_h, wgates.at[1]),
+        ("tokens", tokens_h, token_t.at[rows(tp, mine), :]),
+        ("wi", wi_h, wgates.at[pl.ds(0, n_gate), :]),
+        ("wf", wf_h, wgates.at[pl.ds(n_gate, n_gate), :]),
         ("wq", wq_h, w1.at[:, pl.ds(0, dq)]),
         ("wk", wk_h, w1.at[:, pl.ds(dq, dk)]),
         ("wv", wv_h, w1.at[:, pl.ds(dq + dk, dv)]),
@@ -118,7 +118,6 @@
         ).wait_recv()
 
     loads["tokens"].wait()
-    token_t[rows(tp, mine), :] = tokens[...].astype(F32).T.astype(BF16)
     pl.semaphore_wait(barrier, (n_tp - 1) + (n_y - 1) + 1)
     for d in far_first(n_tp):
         part = token_t.at[rows(tp, mine), :]
@@ -126,14 +125,13 @@
 
     loads["wi"].wait()
     loads["wf"].wait()
-    lane_w = lax.broadcasted_iota(jnp.int32, (n_gate, LANES), 1)
-    row_w = lax.broadcasted_iota(jnp.int32, (n_gate, LANES), 0)
-    low_lane = lax.rem(lane_w, HALF)
-    head_row = row_w - tp * heads
-    pick_i = jnp.where((low_lane == head_row) & (head_row < heads) & (head_row >= 0), 1.0, 0.0).astype(BF16)
-    pick_f = jnp.where((low_lane == head_row + heads) & (head_row < heads) & (head_row >= 0), 1.0, 0.0).astype(BF16)
-    w1[:, n_main:] = (
-        jnp.dot(wgates[0], pick_i, preferred_element_type=F32) + jnp.dot(wgates[1], pick_f, preferred_element_type=F32)
+    lane_w = lax.rem(lax.broadcasted_iota(jnp.int32, (2 * n_gate, LANES), 1), HALF)
+    row_w = lax.broadcasted_iota(jnp.int32, (2 * n_gate, LANES), 0)
+    is_f = row_w // n_gate
+    head = row_w - is_f * n_gate - tp * heads
+    pick = jnp.where((head >= 0) & (head < heads) & (lane_w == head + heads * is_f), 1.0, 0.0).astype(BF16)
+    w1[:, n_main:] = lax.dot_general(
+        wgates[...], pick, (((0,), (0,)), ((), ())), preferred_element_type=F32
     ).astype(BF16)
 
     loads["mix"].wait()
@@ -151,7 +149,7 @@
 
     def project(gain, weights, widths, square_lane, gates, core_of, store):
         wide = x_raw[:, core_of].reshape(half_rows, feats).astype(F32)
-        normed = (wide * gain[...].astype(F32)).astype(BF16)
+        normed = (wide * gain[...].astype(F32)[None, :]).astype(BF16)
         squares = jnp.sum(wide * wide, axis=1, keepdims=True)
         for at, width in widths:
             store(at, width, jnp.dot(normed, weights[:, at : at + width], preferred_element_type=F32))
@@ -255,9 +253,9 @@
     loads["stab"].wait()
     loads["norm"].wait()
     loads["mem"].wait()
-    held = lforget + stab[...]
+    held = lforget + stab[...].T
     new_stab = jnp.maximum(held, igate)
-    newstab_ref[...] = new_stab
+    newstab_ref[...] = new_stab.T
     decay = jnp.exp(held - new_stab)
     inflow = jnp.exp(igate - new_stab)
     floor = jnp.exp(-new_stab)
@@ -340,17 +338,16 @@
             jax.ShapeDtypeStruct((mine, seqs), BF16),
             jax.ShapeDtypeStruct(memory.shape, F32),
             jax.ShapeDtypeStruct(normalizer.shape, F32),
-            jax.ShapeDtypeStruct(stabilizer.shape, F32),
+            jax.ShapeDtypeStruct(stabilizer.shape[::-1], F32),
         ),
         in_specs=[hbm, vmem] + [hbm] * 10 + [vmem] + [hbm] * 3,
         out_specs=(vmem, hbm, vmem, vmem),
         scratch_shapes=[
-            pltpu.VMEM(tokens.shape, BF16),
             pltpu.VMEM((feats, n1), BF16),
-            pltpu.VMEM((2, *w_input_gate.shape), BF16),
+            pltpu.VMEM((2 * w_input_gate.shape[1], feats), BF16),
             pltpu.VMEM(memory.shape, F32),
             pltpu.VMEM(normalizer.shape, F32),
-            pltpu.VMEM(stabilizer.shape, F32),
+            pltpu.VMEM(stabilizer.shape[::-1], F32),
             pltpu.VMEM(w_mix_out.shape, BF16),
             pltpu.VMEM(w_mix_out.shape[::-1], BF16),
             pltpu.VMEM((feats, 2 * n_ff), BF16),
@@ -386,13 +383,13 @@
             ys, ys, ys, ys,
             xs, xs,
         ],
-        compiler_params=pltpu.CompilerParams(collective_id=0, has_side_effects=True, vmem_limit_bytes=48 * 1024 * 1024),
+        compiler_params=pltpu.CompilerParams(collective_id=0, has_side_effects=True, vmem_limit_bytes=67_043_328),
         name="layer",
     )(
-        tokens, norm_gain.reshape(1, -1), w_query, w_key, w_value, w_outgate, w_input_gate, w_forget_gate,
-        memory, normalizer, stabilizer, w_mix_out, ffn_gain.reshape(1, -1), w_gate, w_up, w_down,
+        tokens.T, norm_gain, w_query, w_key, w_value, w_outgate, w_input_gate.T, w_forget_gate.T,
+        memory, normalizer, stabilizer.T, w_mix_out, ffn_gain, w_gate, w_up, w_down,
     )
-    return out_t.T, new_memory, new_normalizer, new_stabilizer
+    return out_t.T, new_memory, new_normalizer, new_stabilizer.T
 
 
 def solution(mesh):

time: 116 us -> 106 us (0.914)
  local copies, waits for them, and re-layouts: 16.5 us -> 5.69 us
    unnamed x26 -> x8, local copies, waits for them, and re-layouts: 15.2 us -> 5.69 us
    reshape x2 -> x0, local copies, waits for them, and re-layouts: 1.32 us -> none  [the longest x1 0.66 us: shards(): norm_gain.reshape(1, -1)]
where the time goes in v2:
time: 106 us
  Pallas kernels  99.6 us (94%)
  local copies, waits for them, and re-layouts  5.69 us (5%)
    pallas_call x1, Pallas kernels, shards(): pl.pallas_call(functools.partial(layer_kernel, n_kv, n_tp), out_shape=(ja...  99.6 us
    unnamed x8, local copies, waits for them, and re-layouts  5.69 us

profile of v2, /device:TPU:513, one launch (start us, length us, event | category | flops | bytes accessed | tf_op | source)
XLA Modules:
  0.0 105.9 jit_solution(9480312879125114465)
XLA Ops:
  0.6 99.6 %layer.1 = (bf16[32,256]{1,0:T(8,128)(2,1)}, f32[16,4,64,128]{3,2,1,0:T(8,128)}, f32[16,4,64]{2,1,0:T(4,128)}, f32[4,16]{1,0:T(4,128)}) custom-call(bf16[32,256]{1,0:T(8,128)(2,1)} %bitcast.6, bf16[256]{0:T(256)(128)(2,1)} %norm_gain.1, bf16[256,256]{1,0:T(8,128)(2,1)} %wq_h.1, bf16[256,256]{1,0:T(8,128)(2,1)} %wk_h.1, bf16[256,512]{1,0:T(8,128)(2,1)} %wv_h.1, ...), custom_call_target="tpu_custom_call" | custom-call | tf_op jit(solution)/shard_map/layer/pallas_call | solution.py:335
  100.2 1.3 %copy.24 = bf16[256,32]{0,1:T(8,128)(2,1)} copy(bf16[256,32]{0,1:T(8,128)(2,1)} %bitcast.9) | data formatting | bytes 32768
  101.6 0.0 copy-start
  101.6 0.0 copy-start.1
  101.6 3.2 %copy.25 = f32[16,4,64,128]{3,2,1,0:T(8,128)} copy(f32[16,4,64,128]{3,2,1,0:T(8,128)} %get-tuple-element.17) | data formatting | bytes 4194304
  104.7 0.0 copy-done
  104.7 0.6 copy.26
  105.4 0.0 copy-done.1
  105.4 0.6 copy.27
Async XLA Ops:
  101.6 3.2 %copy-start = (f32[16,4,64]{2,1,0:T(4,128)S(1)}, f32[16,4,64]{2,1,0:T(4,128)}, u32[]{:S(2)}) copy-start(f32[16,4,64]{2,1,0:T(4,128)} %get-tuple-element.18) | copy-start | bytes 49156
  101.6 3.8 %copy-start.1 = (f32[4,16]{1,0:T(4,128)S(1)}, f32[4,16]{1,0:T(4,128)}, u32[]{:S(2)}) copy-start(f32[4,16]{1,0:T(4,128)} %get-tuple-element.11) | copy-start | bytes 772

commit v3 on v2

--- a/solution.py
+++ b/solution.py
@@ -11,6 +11,7 @@
 DV = 128
 LANES = 128
 HALF = LANES // 2
+FF_CHUNK = 3 * LANES
 F32 = jnp.float32
 BF16 = jnp.bfloat16
 MESH = pl.DeviceIdType.MESH
@@ -26,6 +27,10 @@
 
 def column_pieces(width, step=256):
     return [(at, min(step, width - at)) for at in range(0, width, step)]
+
+
+def ff_chunks(width):
+    return column_pieces(width, FF_CHUNK)
 
 
 def hi_lo(values, lane):
@@ -43,7 +48,7 @@
     out_ref, newmem_h, newnorm_ref, newstab_ref,
     w1, wgates, mem, norm, stab, wmix, wmix_t, w2, wd, wd_t,
     token_t, x_raw, z1_pair, z1_own, z1_got, z1_send, z1_recv,
-    numer, gated, mix_send, mix_recv, mixed_t, z2_pair, z2_own, z2_got, z2_send, z2_recv, hidden, down_send, down_recv,
+    numer, gated, mix_send, mix_recv, mixed_t, z2_pair, z2_own, z2_got, z2_send, z2_recv, hidden, down_sum, down_send, down_recv,
     local_sem, tok_s, tok_r, p1_s, p1_r, a_s, a_r, g_s, g_r, gf_s, gf_r, m_s, m_r, x_s, x_r, p2_s, p2_r, b_s, b_r, h_s, h_r, hf_s, hf_r, d_s, d_r,
 ):
     kv, tp = lax.axis_index("kv"), lax.axis_index("tp")
@@ -98,10 +103,12 @@
         ("mem", mem_h, mem),
         ("norm", norm_h, norm),
         ("stab", stab_h, stab),
-        ("gate", wg_h, w2.at[:, pl.ds(0, n_ff)]),
-        ("up", wu_h, w2.at[:, pl.ds(n_ff, n_ff)]),
+    ) + tuple(
+        (f"{name}{at}", source.at[:, pl.ds(at, size)], w2.at[:, pl.ds(2 * at + shift * size, size)])
+        for at, size in ff_chunks(n_ff)
+        for shift, (name, source) in enumerate((("gate", wg_h), ("up", wu_h)))
     )):
-        loads[name] = pltpu.make_async_copy(source, target, local_sem.at[i])
+        loads[name] = pltpu.make_async_copy(source, target, local_sem.at[i + (i >= 12)])
         loads[name].start()
     sent = []
 
@@ -118,32 +125,35 @@
         ).wait_recv()
 
     loads["tokens"].wait()
-    pl.semaphore_wait(barrier, (n_tp - 1) + (n_y - 1) + 1)
+    with jax.named_scope("barrier"):
+        pl.semaphore_wait(barrier, (n_tp - 1) + (n_y - 1) + 1)
     for d in far_first(n_tp):
         part = token_t.at[rows(tp, mine), :]
         send(part, part, tok_s.at[d], tok_r.at[d], {"tp": tp_of(d)})
 
     loads["wi"].wait()
     loads["wf"].wait()
-    lane_w = lax.rem(lax.broadcasted_iota(jnp.int32, (2 * n_gate, LANES), 1), HALF)
-    row_w = lax.broadcasted_iota(jnp.int32, (2 * n_gate, LANES), 0)
-    is_f = row_w // n_gate
-    head = row_w - is_f * n_gate - tp * heads
-    pick = jnp.where((head >= 0) & (head < heads) & (lane_w == head + heads * is_f), 1.0, 0.0).astype(BF16)
-    w1[:, n_main:] = lax.dot_general(
-        wgates[...], pick, (((0,), (0,)), ((), ())), preferred_element_type=F32
-    ).astype(BF16)
-
-    loads["mix"].wait()
-    wmix_t[...] = wmix[...].T
-    loads["down"].wait()
-    for at, width in column_pieces(wd.shape[0]):
-        wd_t[:, at : at + width] = wd[at : at + width, :].T
-    for name in ("wq", "wk", "wv", "wo"):
-        loads[name].wait()
-
-    for d in near_first(n_tp):
-        arrive(token_t.at[rows(from_tp(d), mine), :], tok_s.at[d], tok_r.at[d], {"tp": tp_of(d)})
+    with jax.named_scope("prep"):
+        lane_w = lax.rem(lax.broadcasted_iota(jnp.int32, (2 * n_gate, LANES), 1), HALF)
+        row_w = lax.broadcasted_iota(jnp.int32, (2 * n_gate, LANES), 0)
+        is_f = row_w // n_gate
+        head = row_w - is_f * n_gate - tp * heads
+        pick = jnp.where((head >= 0) & (head < heads) & (lane_w == head + heads * is_f), 1.0, 0.0).astype(BF16)
+        w1[:, n_main:] = lax.dot_general(
+            wgates[...], pick, (((0,), (0,)), ((), ())), preferred_element_type=F32
+        ).astype(BF16)
+
+        loads["mix"].wait()
+        wmix_t[...] = wmix[...].T
+        loads["down"].wait()
+        for at, width in column_pieces(wd.shape[0]):
+            wd_t[:, at : at + width] = wd[at : at + width, :].T
+        for name in ("wq", "wk", "wv", "wo"):
+            loads[name].wait()
+
+    with jax.named_scope("wait_tok"):
+        for d in near_first(n_tp):
+            arrive(token_t.at[rows(from_tp(d), mine), :], tok_s.at[d], tok_r.at[d], {"tp": tp_of(d)})
 
     lane = lax.broadcasted_iota(jnp.int32, (half_rows, LANES), 1)
 
@@ -171,30 +181,34 @@
         def keep(at, size, z):
             own_z[:, :, at : at + size] = z.reshape(n_y, own, size)
 
-        project(gain, weights, pieces, square_lane, gates, other, to_partner)
-        send(pair, got, p_s, p_r, {"kv": partner})
-        project(gain, weights, pieces, square_lane, gates, core, keep)
-        arrive(got, p_s, p_r, {"kv": partner})
+        with jax.named_scope("proj"):
+            project(gain, weights, pieces, square_lane, gates, other, to_partner)
+            send(pair, got, p_s, p_r, {"kv": partner})
+            project(gain, weights, pieces, square_lane, gates, core, keep)
+        with jax.named_scope("wait_pair"):
+            arrive(got, p_s, p_r, {"kv": partner})
         small_lane = lax.broadcasted_iota(jnp.int32, (own, LANES), 1)
-        for d in far_first(n_y) + [0]:
-            at_y = y_of(d)
-            for at, size in pieces + [(width, LANES)]:
-                both = own_z[at_y, :, at : at + size]
-                other_half = got[at_y, :, at : at + size].astype(F32)
-                if at == width:
-                    both = both + (other_half + jnp.concatenate([other_half[:, HALF:], other_half[:, :HALF]], axis=1))
+        with jax.named_scope("pairsum"):
+            for d in far_first(n_y) + [0]:
+                at_y = y_of(d)
+                for at, size in pieces + [(width, LANES)]:
+                    both = own_z[at_y, :, at : at + size]
+                    other_half = got[at_y, :, at : at + size].astype(F32)
+                    if at == width:
+                        both = both + (other_half + jnp.concatenate([other_half[:, HALF:], other_half[:, :HALF]], axis=1))
+                        if d:
+                            both = hi_lo(both, small_lane)
+                    else:
+                        both = both + other_half
                     if d:
-                        both = hi_lo(both, small_lane)
-                else:
-                    both = both + other_half
+                        out[d, :, at : at + size] = both.astype(BF16)
+                    else:
+                        total_at[:, at : at + size] = both
                 if d:
-                    out[d, :, at : at + size] = both.astype(BF16)
-                else:
-                    total_at[:, at : at + size] = both
-            if d:
-                send(out.at[d], into.at[d], r_s.at[d], r_r.at[d], {"kv": 2 * at_y + core})
-        for d in near_first(n_y):
-            arrive(into.at[d], r_s.at[d], r_r.at[d], {"kv": 2 * y_of(d) + core})
+                    send(out.at[d], into.at[d], r_s.at[d], r_r.at[d], {"kv": 2 * at_y + core})
+        with jax.named_scope("wait_rs"):
+            for d in near_first(n_y):
+                arrive(into.at[d], r_s.at[d], r_r.at[d], {"kv": 2 * y_of(d) + core})
 
     def total_of(total_at, into, at, size):
         value = total_at[:, at : at + size]
@@ -241,81 +255,251 @@
     reduce_over_kv(
         norm_gain, w1, n_main, 2 * heads, True, z1_pair, z1_own, z1_got, z1_send, z1_recv, (p1_s, p1_r, a_s, a_r), z_total
     )
-    gates = tile_of(z_total, z1_recv, n_main)
-    scale1 = lax.rsqrt(gates[:, 2 * heads : 2 * heads + 1] / n_feats + 1e-06)
-    query = scale1 * total_of(z_total, z1_recv, 0, dq) * DQK ** (-0.5)
-    key = scale1 * total_of(z_total, z1_recv, dq, dk)
-    value = scale1 * total_of(z_total, z1_recv, dq + dk, dv)
-    outgate = scale1 * total_of(z_total, z1_recv, dq + dk + dv, dv)
-    igate = scale1 * gates[:, :heads]
-    forget = scale1 * gates[:, heads : 2 * heads]
-    lforget = jnp.minimum(forget, 0.0) - jnp.log1p(jnp.exp(-jnp.abs(forget)))
-    loads["stab"].wait()
-    loads["norm"].wait()
-    loads["mem"].wait()
-    held = lforget + stab[...].T
-    new_stab = jnp.maximum(held, igate)
-    newstab_ref[...] = new_stab.T
-    decay = jnp.exp(held - new_stab)
-    inflow = jnp.exp(igate - new_stab)
-    floor = jnp.exp(-new_stab)
-    query_t = query.T
-    for s in range(own):
+    with jax.named_scope("gates"):
+        gates = tile_of(z_total, z1_recv, n_main)
+        scale1 = lax.rsqrt(gates[:, 2 * heads : 2 * heads + 1] / n_feats + 1e-06)
+        query = scale1 * total_of(z_total, z1_recv, 0, dq) * DQK ** (-0.5)
+        key = scale1 * total_of(z_total, z1_recv, dq, dk)
+        value = scale1 * total_of(z_total, z1_recv, dq + dk, dv)
+        outgate = scale1 * total_of(z_total, z1_recv, dq + dk + dv, dv)
+        igate = scale1 * gates[:, :heads]
+        forget = scale1 * gates[:, heads : 2 * heads]
+        lforget = jnp.minimum(forget, 0.0) - jnp.log1p(jnp.exp(-jnp.abs(forget)))
+        loads["stab"].wait()
+        loads["norm"].wait()
+        loads["mem"].wait()
+        held = lforget + stab[...].T
+        new_stab = jnp.maximum(held, igate)
+        newstab_ref[...] = new_stab.T
+        decay = jnp.exp(held - new_stab)
+        inflow = jnp.exp(igate - new_stab)
+        floor = jnp.exp(-new_stab)
+    with jax.named_scope("readout"):
+        query_t = query.T
+        for s in range(own):
+            for h in range(heads):
+                column = query_t[h * DQK : (h + 1) * DQK, s : s + 1]
+                numer[s : s + 1, h * DV : (h + 1) * DV] = jnp.sum(column * mem[s, h], axis=0, keepdims=True)
+    with jax.named_scope("norm"):
         for h in range(heads):
-            column = query_t[h * DQK : (h + 1) * DQK, s : s + 1]
-            numer[s : s + 1, h * DV : (h + 1) * DV] = jnp.sum(column * mem[s, h], axis=0, keepdims=True)
-    for h in range(heads):
-        q, k = query[:, h * DQK : (h + 1) * DQK], key[:, h * DQK : (h + 1) * DQK]
-        keep, add = decay[:, h : h + 1], inflow[:, h : h + 1]
-        new_norm = keep * norm[:, h, :] + add * k
-        newnorm_ref[:, h, :] = new_norm
-        denom = jnp.maximum(jnp.abs(jnp.sum(q * new_norm, axis=1, keepdims=True)), floor[:, h : h + 1])
-        at = slice(h * DV, (h + 1) * DV)
-        top = keep * numer[:, at] + (add * jnp.sum(q * k, axis=1, keepdims=True)) * value[:, at]
-        gated[rows(kv, own), at] = (jax.nn.sigmoid(outgate[:, at]) * (top / denom)).astype(BF16)
+            q, k = query[:, h * DQK : (h + 1) * DQK], key[:, h * DQK : (h + 1) * DQK]
+            keep, add = decay[:, h : h + 1], inflow[:, h : h + 1]
+            new_norm = keep * norm[:, h, :] + add * k
+            newnorm_ref[:, h, :] = new_norm
+            denom = jnp.maximum(jnp.abs(jnp.sum(q * new_norm, axis=1, keepdims=True)), floor[:, h : h + 1])
+            at = slice(h * DV, (h + 1) * DV)
+            top = keep * numer[:, at] + (add * jnp.sum(q * k, axis=1, keepdims=True)) * value[:, at]
+            gated[rows(kv, own), at] = (jax.nn.sigmoid(outgate[:, at]) * (top / denom)).astype(BF16)
     finish = gather_over_kv(gated, (g_s, g_r, gf_s, gf_r))
 
-    spread = jnp.concatenate([jnp.broadcast_to(inflow[:, h : h + 1], (own, DQK)) for h in range(heads)], axis=1)
-    key_t = (key * spread).T
-    for s in range(own):
-        for h in range(heads):
-            column = key_t[h * DQK : (h + 1) * DQK, s : s + 1]
-            mem[s, h] = decay[s : s + 1, h : h + 1] * mem[s, h] + column * value[s : s + 1, h * DV : (h + 1) * DV]
-    put = pltpu.make_async_copy(mem, newmem_h, local_sem.at[14])
+    with jax.named_scope("newmem"):
+        spread = jnp.concatenate([jnp.broadcast_to(inflow[:, h : h + 1], (own, DQK)) for h in range(heads)], axis=1)
+        key_t = (key * spread).T
+        for s in range(own):
+            for h in range(heads):
+                column = key_t[h * DQK : (h + 1) * DQK, s : s + 1]
+                mem[s, h] = decay[s : s + 1, h : h + 1] * mem[s, h] + column * value[s : s + 1, h * DV : (h + 1) * DV]
+    put = pltpu.make_async_copy(mem, newmem_h, local_sem.at[12])
     put.start()
-    finish()
-
-    partial = lax.dot_general(wmix_t[...], gated[...], (((1,), (1,)), ((), ())), preferred_element_type=F32)
-    total = sum_over_tp(partial, mix_send, mix_recv, (m_s, m_r))
+    with jax.named_scope("wait_gated"):
+        finish()
+
+    with jax.named_scope("mixdot"):
+        partial = lax.dot_general(wmix_t[...], gated[...], (((1,), (1,)), ((), ())), preferred_element_type=F32)
+    with jax.named_scope("mixrs"):
+        total = sum_over_tp(partial, mix_send, mix_recv, (m_s, m_r))
     mixed = (token_t[rows(tp, mine), :].astype(F32) + total).astype(BF16)
     mixed_t[rows(tp, mine), :] = mixed
     for d in far_first(n_tp):
         part = mixed_t.at[rows(tp, mine), :]
         send(part, part, x_s.at[d], x_r.at[d], {"tp": tp_of(d)})
-    loads["gate"].wait()
-    loads["up"].wait()
-    for d in near_first(n_tp):
-        arrive(mixed_t.at[rows(from_tp(d), mine), :], x_s.at[d], x_r.at[d], {"tp": tp_of(d)})
-
-    u_total = z2_own.at[y]
+    with jax.named_scope("wait_mixed"):
+        for at, _ in ff_chunks(n_ff):
+            loads[f"gate{at}"].wait()
+            loads[f"up{at}"].wait()
+        for d in near_first(n_tp):
+            arrive(mixed_t.at[rows(from_tp(d), mine), :], x_s.at[d], x_r.at[d], {"tp": tp_of(d)})
+
     x_raw[...] = mixed_t[...].T.reshape(x_raw.shape)
-    reduce_over_kv(
-        ffn_gain, w2, 2 * n_ff, 0, False, z2_pair, z2_own, z2_got, z2_send, z2_recv, (p2_s, p2_r, b_s, b_r), u_total
-    )
-    squares = tile_of(u_total, z2_recv, 2 * n_ff)[:, :1]
-    scale2 = lax.rsqrt(squares / n_feats + 1e-06)
-    for at, size in column_pieces(n_ff):
-        gate = scale2 * total_of(u_total, z2_recv, at, size)
-        up = scale2 * total_of(u_total, z2_recv, n_ff + at, size)
-        hidden[rows(kv, own), at : at + size] = (gate * jax.nn.sigmoid(gate) * up).astype(BF16)
-    gather_over_kv(hidden, (h_s, h_r, hf_s, hf_r))()
-
-    partial = lax.dot_general(wd_t[...], hidden[...], (((1,), (1,)), ((), ())), preferred_element_type=F32)
-    total = sum_over_tp(partial, down_send, down_recv, (d_s, d_r))
+    chunks = ff_chunks(n_ff)
+    order = [len(chunks) - 1] + list(range(len(chunks) - 1))
+    wide_lane = lax.broadcasted_iota(jnp.int32, (half_rows, LANES), 1)
+    small_lane = lax.broadcasted_iota(jnp.int32, (own, LANES), 1)
+
+    def project_chunks(core_of, ours):
+        wide = x_raw[:, core_of].reshape(half_rows, feats).astype(F32)
+        normed = (wide * ffn_gain[...].astype(F32)[None, :]).astype(BF16)
+        squares = jnp.sum(wide * wide, axis=1, keepdims=True)
+        tile = jnp.broadcast_to(squares, (half_rows, LANES))
+        if ours:
+            z2_own[:, :, 2 * n_ff :] = tile.reshape(n_y, own, LANES)
+        else:
+            z2_pair[:, :, 2 * n_ff :] = hi_lo(tile, wide_lane).reshape(n_y, own, LANES)
+        for c in order:
+            at, size = chunks[c]
+            for start in (2 * at, 2 * at + size):
+                z = jnp.dot(normed, w2[:, start : start + size], preferred_element_type=F32)
+                if ours:
+                    z2_own[:, :, start : start + size] = z.reshape(n_y, own, size)
+                else:
+                    z2_pair[:, :, start : start + size] = z.astype(BF16).reshape(n_y, own, size)
+            if not ours:
+                part = pl.ds(2 * at, width_of(c))
+                send(z2_pair.at[:, :, part], z2_got.at[:, :, part], p2_s.at[c], p2_r.at[c], {"kv": partner})
+
+    def width_of(c):
+        return 2 * chunks[c][1] + (LANES if c == len(chunks) - 1 else 0)
+
+    def spans(c):
+        at, size = chunks[c]
+        return [(2 * at, size, False), (2 * at + size, size, False)] + (
+            [(2 * n_ff, LANES, True)] if c == len(chunks) - 1 else []
+        )
+
+    def plain(tile, is_square):
+        tile = tile.astype(F32)
+        if is_square:
+            tile = tile + jnp.concatenate([tile[:, HALF:], tile[:, :HALF]], axis=1)
+        return tile
+
+    def add_up(c, dest, received, put):
+        for at, size, is_square in spans(c):
+            value = z2_own[dest, :, at : at + size] + plain(z2_got[dest, :, at : at + size], is_square)
+            for slot in received:
+                value = value + plain(z2_recv[slot, :, at : at + size], is_square)
+            put(at, size, is_square, value)
+
+    def pass_on(c, dest, received, slot, hops):
+        def put(at, size, is_square, value):
+            z2_send[slot, :, at : at + size] = hi_lo(value, small_lane) if is_square else value.astype(BF16)
+
+        add_up(c, dest, received, put)
+        part = pl.ds(2 * chunks[c][0], width_of(c))
+        where = {"kv": 2 * lax.rem(y + n_y + hops, n_y) + core}
+        send(z2_send.at[slot, :, part], z2_recv.at[slot, :, part], b_s.at[slot, c], b_r.at[slot, c], where)
+
+    def take(c, slot):
+        part = pl.ds(2 * chunks[c][0], width_of(c))
+        target = z2_recv.at[slot, :, part]
+        arrive(target, b_s.at[slot, c], b_r.at[slot, c], {"kv": partner})
+
+    far, short = n_y // 2, n_y // 2 - 1
+    with jax.named_scope("proj2a"):
+        project_chunks(other, False)
+    with jax.named_scope("proj2b"):
+        project_chunks(core, True)
+
+    def way(c):
+        return 1 if c % 2 == 0 else -1
+
+    def slot_of(sign, step):
+        return step if sign == 1 else short + step
+
+    for c in order:
+        with jax.named_scope(f"ring#s=1#c={c}"):
+            part = pl.ds(2 * chunks[c][0], width_of(c))
+            arrive(z2_got.at[:, :, part], p2_s.at[c], p2_r.at[c], {"kv": partner})
+            pass_on(c, lax.rem(y + far, n_y), [], 0, 2 * way(c))
+            for sign in (1, -1):
+                pass_on(c, lax.rem(y + n_y + sign * short, n_y), [], slot_of(sign, 1), sign)
+    for step in range(2, short + 1):
+        for c in order:
+            with jax.named_scope(f"ring#s={step}#c={c}"):
+                for sign in (-way(c), way(c)):
+                    received = [slot_of(sign, step - 1)]
+                    if step == 2 and sign == way(c):
+                        received.append(0)
+                    for slot in received:
+                        take(c, slot)
+                    pass_on(c, lax.rem(y + n_y + sign * (short + 1 - step), n_y), received, slot_of(sign, step), sign)
+
+    scale2 = None
+    for c in order:
+        at, size = chunks[c]
+        with jax.named_scope(f"hidden#c={c}"):
+            parts = []
+            received = [slot_of(sign, short) for sign in (1, -1)]
+            for slot in received:
+                take(c, slot)
+            add_up(c, y, received, lambda at, size, is_square, value: parts.append(value))
+            if scale2 is None:
+                scale2 = lax.rsqrt(parts[2][:, :1] / n_feats + 1e-06)
+            gate, up = scale2 * parts[0], scale2 * parts[1]
+            hidden[rows(kv, own), at : at + size] = (gate * jax.nn.sigmoid(gate) * up).astype(BF16)
+            part = hidden.at[rows(kv, own), pl.ds(at, size)]
+            for d in far_first(n_y):
+                send(part, part, h_s.at[d, c], h_r.at[d, c], {"kv": 2 * y_of(d) + core})
+            send(part, part, hf_s.at[0, c], hf_r.at[0, c], {"kv": partner})
+
+    def pass_to_partner(c):
+        at, size = chunks[c]
+        with jax.named_scope(f"pass#c={c}"):
+            for d in near_first(n_y):
+                got = hidden.at[rows(2 * from_y(d) + core, own), pl.ds(at, size)]
+                arrive(got, h_s.at[d, c], h_r.at[d, c], {"kv": 2 * y_of(d) + core})
+                send(got, got, hf_s.at[d, c], hf_r.at[d, c], {"kv": partner})
+
+    def down_part(c):
+        at, size = chunks[c]
+        with jax.named_scope(f"down#c={c}"):
+            for d in [0] + near_first(n_y):
+                target = hidden.at[rows(2 * from_y(d) + other, own), pl.ds(at, size)]
+                arrive(target, hf_s.at[d, c], hf_r.at[d, c], {"kv": partner})
+            return lax.dot_general(
+                wd_t[:, at : at + size], hidden[:, at : at + size], (((1,), (1,)), ((), ())), preferred_element_type=F32
+            )
+
+    pass_to_partner(order[0])
+    for i, c in enumerate(order):
+        if i + 1 < len(order):
+            pass_to_partner(order[i + 1])
+        product = down_part(c)
+        if i == 0:
+            down_sum[...] = product
+        elif i + 1 < len(order):
+            down_sum[...] += product
+    with jax.named_scope("downrs"):
+        total = sum_over_tp(down_sum[...] + product, down_send, down_recv, (d_s, d_r))
     out_ref[...] = (mixed_t[rows(tp, mine), :].astype(F32) + total).astype(BF16)
     put.wait()
     for copy in sent:
         copy.wait_send()
+
+
+def copy_kernel(pieces, *refs):
+    count = len(pieces)
+    sources, targets, held, sem = refs[:count], refs[count : 2 * count], refs[2 * count : 3 * count], refs[3 * count]
+    steps, at = [], 0
+    for source, target, buffer, n in zip(sources, targets, held, pieces):
+        size = source.shape[0] // n
+        for i in range(n):
+            part = pl.ds(i * size, size)
+            steps.append((
+                pltpu.make_async_copy(source.at[part], buffer.at[part], sem.at[0, at]),
+                pltpu.make_async_copy(buffer.at[part], target.at[part], sem.at[1, at]),
+            ))
+            at += 1
+    for take, _ in steps:
+        take.start()
+    for take, put in steps:
+        take.wait()
+        put.start()
+    for _, put in steps:
+        put.wait()
+
+
+def hand_over(*arrays):
+    pieces = [4 if a.ndim == 4 else 1 for a in arrays]
+    hbm = pl.BlockSpec(memory_space=pltpu.HBM)
+    return pl.pallas_call(
+        functools.partial(copy_kernel, pieces),
+        out_shape=tuple(jax.ShapeDtypeStruct(a.shape, a.dtype) for a in arrays),
+        in_specs=[hbm] * len(arrays),
+        out_specs=(hbm,) * len(arrays),
+        scratch_shapes=[pltpu.VMEM(a.shape, a.dtype) for a in arrays] + [pltpu.SemaphoreType.DMA((2, sum(pieces)))],
+        compiler_params=pltpu.CompilerParams(vmem_limit_bytes=67_043_328),
+        name="hand_over",
+    )(*arrays)
 
 
 def shards(n_kv, n_tp, tokens, norm_gain, w_query, w_key, w_value, w_outgate, w_input_gate, w_forget_gate, memory, normalizer, stabilizer, w_mix_out, ffn_gain, w_gate, w_up, w_down):
@@ -331,7 +515,8 @@
     hbm = pl.BlockSpec(memory_space=pltpu.HBM)
     vmem = pl.BlockSpec(memory_space=pltpu.VMEM)
     dma = pltpu.SemaphoreType.DMA
-    ys, xs, one = dma((n_y,)), dma((n_tp,)), dma
+    n_chunks = len(ff_chunks(n_ff))
+    ys, xs, one, per_chunk = dma((n_y,)), dma((n_tp,)), dma, dma((n_y, n_chunks))
     out_t, new_memory, new_normalizer, new_stabilizer = pl.pallas_call(
         functools.partial(layer_kernel, n_kv, n_tp),
         out_shape=(
@@ -371,16 +556,17 @@
             pltpu.VMEM((n_y, own, n2), BF16),
             pltpu.VMEM((n_y, own, n2), BF16),
             pltpu.VMEM((seqs, n_ff), BF16),
+            pltpu.VMEM((out_feats, seqs), F32),
             pltpu.VMEM((n_tp, mine, seqs), BF16),
             pltpu.VMEM((n_tp, mine, seqs), BF16),
-            dma((15,)),
+            dma((13 + 2 * len(ff_chunks(n_ff)),)),
             xs, xs,
             one, one, ys, ys,
             ys, ys, ys, ys,
             xs, xs,
             xs, xs,
-            one, one, ys, ys,
-            ys, ys, ys, ys,
+            dma((n_chunks,)), dma((n_chunks,)), per_chunk, per_chunk,
+            per_chunk, per_chunk, per_chunk, per_chunk,
             xs, xs,
         ],
         compiler_params=pltpu.CompilerParams(collective_id=0, has_side_effects=True, vmem_limit_bytes=67_043_328),
@@ -389,6 +575,7 @@
         tokens.T, norm_gain, w_query, w_key, w_value, w_outgate, w_input_gate.T, w_forget_gate.T,
         memory, normalizer, stabilizer.T, w_mix_out, ffn_gain, w_gate, w_up, w_down,
     )
+    out_t, new_memory, new_normalizer, new_stabilizer = hand_over(out_t, new_memory, new_normalizer, new_stabilizer)
     return out_t.T, new_memory, new_normalizer, new_stabilizer.T
 
 

time: 106 us -> 95.7 us (0.903)
  local copies, waits for them, and re-layouts: 5.69 us -> 0 us
  Pallas kernels: 99.6 us -> 94.8 us
    pallas_call x1, Pallas kernels: 99.6 us -> 92.3 us  [shards(): pl.pallas_call(functools.partial(layer_kernel, n_kv, n_tp), out_shape=(ja...]
    unnamed x8 -> x0, local copies, waits for them, and re-layouts: 5.69 us -> none
    pallas_call x0 -> x1, Pallas kernels: none -> 2.5 us  [hand_over(): pl.pallas_call(functools.partial(copy_kernel, pieces), out_shape=tuple((j...]
where the time goes in v3:
time: 95.7 us; the launch traced here: 95.4 us
  Pallas kernels  94.8 us (99%)
    pallas_call x1, Pallas kernels, shards(): pl.pallas_call(functools.partial(layer_kernel, n_kv, n_tp), out_shape=(ja...  92.3 us
    pallas_call x1, Pallas kernels, hand_over(): pl.pallas_call(functools.partial(copy_kernel, pieces), out_shape=tuple((j...  2.5 us

profile of v3, /device:TPU:513, one launch (start us, length us, event | category | flops | bytes accessed | tf_op | source)
XLA Modules:
  0.0 95.4 jit_solution(17195593241020185802)
XLA Ops:
  0.6 92.3 %layer.1 = (bf16[32,256]{1,0:T(8,128)(2,1)}, f32[16,4,64,128]{3,2,1,0:T(8,128)}, f32[16,4,64]{2,1,0:T(4,128)}, f32[4,16]{1,0:T(4,128)}) custom-call(bf16[32,256]{1,0:T(8,128)(2,1)} %bitcast.6, bf16[256]{0:T(256)(128)(2,1)} %norm_gain.1, bf16[256,256]{1,0:T(8,128)(2,1)} %wq_h.1, bf16[256,256]{1,0:T(8,128)(2,1)} %wk_h.1, bf16[256,512]{1,0:T(8,128)(2,1)} %wv_h.1, ...), custom_call_target="tpu_custom_call" | custom-call | tf_op jit(solution)/shard_map/layer/pallas_call | solution.py:520
  92.9 2.5 %hand_over.1 = (bf16[32,256]{1,0:T(8,128)(2,1)}, f32[16,4,64,128]{3,2,1,0:T(8,128)}, f32[16,4,64]{2,1,0:T(4,128)}, f32[4,16]{1,0:T(4,128)}) custom-call(bf16[32,256]{1,0:T(8,128)(2,1)} %get-tuple-element.12.refs_0_, f32[16,4,64,128]{3,2,1,0:T(8,128)} %get-tuple-element.13.refs_1_, f32[16,4,64]{2,1,0:T(4,128)} %get-tuple-element.14.refs_2_, ...), custom_call_target="tpu_custom_call" | custom-call | tf_op jit(solution)/shard_map/hand_over/pallas_call | solution.py:494

commit v4 on v3

--- a/solution.py
+++ b/solution.py
@@ -30,16 +30,24 @@
 
 
 def ff_chunks(width):
-    return column_pieces(width, FF_CHUNK)
+    first = width % FF_CHUNK or FF_CHUNK
+    return [(0, first)] + [(at, FF_CHUNK) for at in range(first, width, FF_CHUNK)]
+
+
+def with_ends(sizes_of_chunks):
+    at, chunks = 0, []
+    for sizes in sizes_of_chunks:
+        chunk = []
+        for size in sizes:
+            chunk.append((at, size))
+            at += size
+        chunks.append(chunk)
+    return chunks
 
 
 def hi_lo(values, lane):
     high = values.astype(BF16).astype(F32)
     return jnp.where(lane < HALF, high, values - high).astype(BF16)
-
-
-def from_hi_lo(tile):
-    return tile[:, :HALF] + tile[:, HALF:]
 
 
 def layer_kernel(
@@ -86,7 +94,6 @@
     pl.semaphore_signal(barrier, inc=1, device_id={"kv": partner}, device_id_type=MESH)
 
     dq, dk, dv = wq_h.shape[1], wk_h.shape[1], wv_h.shape[1]
-    n_main = dq + dk + 2 * dv
     n_ff = wg_h.shape[1]
     n_gate = wi_h.shape[0]
     loads = {}
@@ -94,17 +101,17 @@
         ("tokens", tokens_h, token_t.at[rows(tp, mine), :]),
         ("wi", wi_h, wgates.at[pl.ds(0, n_gate), :]),
         ("wf", wf_h, wgates.at[pl.ds(n_gate, n_gate), :]),
-        ("wq", wq_h, w1.at[:, pl.ds(0, dq)]),
-        ("wk", wk_h, w1.at[:, pl.ds(dq, dk)]),
-        ("wv", wv_h, w1.at[:, pl.ds(dq + dk, dv)]),
-        ("wo", wo_h, w1.at[:, pl.ds(dq + dk + dv, dv)]),
+        ("wq", wq_h, w1.at[:, pl.ds(LANES, dq)]),
+        ("wk", wk_h, w1.at[:, pl.ds(LANES + dq, dk)]),
+        ("wv", wv_h, w1.at[:, pl.ds(LANES + dq + dk, dv)]),
+        ("wo", wo_h, w1.at[:, pl.ds(LANES + dq + dk + dv, dv)]),
         ("mix", wmix_h, wmix),
         ("down", wd_h, wd),
         ("mem", mem_h, mem),
         ("norm", norm_h, norm),
         ("stab", stab_h, stab),
     ) + tuple(
-        (f"{name}{at}", source.at[:, pl.ds(at, size)], w2.at[:, pl.ds(2 * at + shift * size, size)])
+        (f"{name}{at}", source.at[:, pl.ds(at, size)], w2.at[:, pl.ds(LANES + 2 * at + shift * size, size)])
         for at, size in ff_chunks(n_ff)
         for shift, (name, source) in enumerate((("gate", wg_h), ("up", wu_h)))
     )):
@@ -139,7 +146,7 @@
         is_f = row_w // n_gate
         head = row_w - is_f * n_gate - tp * heads
         pick = jnp.where((head >= 0) & (head < heads) & (lane_w == head + heads * is_f), 1.0, 0.0).astype(BF16)
-        w1[:, n_main:] = lax.dot_general(
+        w1[:, :LANES] = lax.dot_general(
             wgates[...], pick, (((0,), (0,)), ((), ())), preferred_element_type=F32
         ).astype(BF16)
 
@@ -157,70 +164,92 @@
 
     lane = lax.broadcasted_iota(jnp.int32, (half_rows, LANES), 1)
 
-    def project(gain, weights, widths, square_lane, gates, core_of, store):
-        wide = x_raw[:, core_of].reshape(half_rows, feats).astype(F32)
-        normed = (wide * gain[...].astype(F32)[None, :]).astype(BF16)
-        squares = jnp.sum(wide * wide, axis=1, keepdims=True)
-        for at, width in widths:
-            store(at, width, jnp.dot(normed, weights[:, at : at + width], preferred_element_type=F32))
-        end = widths[-1][0] + widths[-1][1]
-        tile = jnp.broadcast_to(squares, (half_rows, LANES))
-        if gates:
-            last = jnp.dot(normed, weights[:, end : end + LANES], preferred_element_type=F32)
-            tile = jnp.where(lax.rem(lane, HALF) == square_lane, tile, last)
-        store(end, LANES, tile)
-
-    def reduce_over_kv(gain, weights, width, square_lane, gates, pair, own_z, got, out, into, sems, total_at):
+    small_lane = lax.broadcasted_iota(jnp.int32, (own, LANES), 1)
+    far, short = n_y // 2, n_y // 2 - 1
+
+    def slot_of(sign, step):
+        return step if sign == 1 else short + step
+
+    def sum_over_kv(name, gain, weights, square_lane, chunks, pair, own_z, got, out, into, sems):
         p_s, p_r, r_s, r_r = sems
-        pieces = column_pieces(width)
-
-        def to_partner(at, size, z):
-            value = hi_lo(z, lane) if at == width else z.astype(BF16)
-            pair[:, :, at : at + size] = value.reshape(n_y, own, size)
-
-        def keep(at, size, z):
-            own_z[:, :, at : at + size] = z.reshape(n_y, own, size)
-
-        with jax.named_scope("proj"):
-            project(gain, weights, pieces, square_lane, gates, other, to_partner)
-            send(pair, got, p_s, p_r, {"kv": partner})
-            project(gain, weights, pieces, square_lane, gates, core, keep)
-        with jax.named_scope("wait_pair"):
-            arrive(got, p_s, p_r, {"kv": partner})
-        small_lane = lax.broadcasted_iota(jnp.int32, (own, LANES), 1)
-        with jax.named_scope("pairsum"):
-            for d in far_first(n_y) + [0]:
-                at_y = y_of(d)
-                for at, size in pieces + [(width, LANES)]:
-                    both = own_z[at_y, :, at : at + size]
-                    other_half = got[at_y, :, at : at + size].astype(F32)
-                    if at == width:
-                        both = both + (other_half + jnp.concatenate([other_half[:, HALF:], other_half[:, :HALF]], axis=1))
-                        if d:
-                            both = hi_lo(both, small_lane)
+
+        def part_of(c):
+            return pl.ds(chunks[c][0][0], sum(size for _, size in chunks[c]))
+
+        def project(core_of, ours):
+            wide = x_raw[:, core_of].reshape(half_rows, feats).astype(F32)
+            normed = (wide * gain[...].astype(F32)[None, :]).astype(BF16)
+            squares = jnp.sum(wide * wide, axis=1, keepdims=True)
+            for c, chunk in enumerate(chunks):
+                for at, size in chunk:
+                    if at == 0 and square_lane is None:
+                        z = jnp.broadcast_to(squares, (half_rows, LANES))
                     else:
-                        both = both + other_half
-                    if d:
-                        out[d, :, at : at + size] = both.astype(BF16)
+                        z = jnp.dot(normed, weights[:, at : at + size], preferred_element_type=F32)
+                        if at == 0:
+                            z = jnp.where(lax.rem(lane, HALF) == square_lane, squares, z)
+                    if ours:
+                        own_z[:, :, at : at + size] = z.reshape(n_y, own, size)
                     else:
-                        total_at[:, at : at + size] = both
-                if d:
-                    send(out.at[d], into.at[d], r_s.at[d], r_r.at[d], {"kv": 2 * at_y + core})
-        with jax.named_scope("wait_rs"):
-            for d in near_first(n_y):
-                arrive(into.at[d], r_s.at[d], r_r.at[d], {"kv": 2 * y_of(d) + core})
-
-    def total_of(total_at, into, at, size):
-        value = total_at[:, at : at + size]
-        for d in range(1, n_y):
-            value = value + into[d, :, at : at + size].astype(F32)
-        return value
-
-    def tile_of(total_at, into, at):
-        rest = into[1, :, at : at + LANES].astype(F32)
-        for d in range(2, n_y):
-            rest = rest + into[d, :, at : at + LANES].astype(F32)
-        return total_at[:, at : at + HALF] + from_hi_lo(rest)
+                        z = hi_lo(z, lane) if at == 0 else z.astype(BF16)
+                        pair[:, :, at : at + size] = z.reshape(n_y, own, size)
+                if not ours:
+                    send(pair.at[:, :, part_of(c)], got.at[:, :, part_of(c)], p_s.at[c], p_r.at[c], {"kv": partner})
+
+        def plain(tile, at):
+            tile = tile.astype(F32)
+            if at == 0:
+                tile = tile + jnp.concatenate([tile[:, HALF:], tile[:, :HALF]], axis=1)
+            return tile
+
+        def add_up(c, dest, received):
+            for at, size in chunks[c]:
+                value = own_z[dest, :, at : at + size] + plain(got[dest, :, at : at + size], at)
+                for slot in received:
+                    value = value + plain(into[slot, :, at : at + size], at)
+                yield at, size, value
+
+        def pass_on(c, dest, received, slot, hops):
+            for at, size, value in add_up(c, dest, received):
+                out[slot, :, at : at + size] = hi_lo(value, small_lane) if at == 0 else value.astype(BF16)
+            where = {"kv": 2 * lax.rem(y + n_y + hops, n_y) + core}
+            send(out.at[slot, :, part_of(c)], into.at[slot, :, part_of(c)], r_s.at[slot, c], r_r.at[slot, c], where)
+
+        def take(c, slot):
+            arrive(into.at[slot, :, part_of(c)], r_s.at[slot, c], r_r.at[slot, c], {"kv": partner})
+
+        def way(c):
+            return 1 if c % 2 == 0 else -1
+
+        with jax.named_scope(f"{name}_proj_a"):
+            project(other, False)
+        with jax.named_scope(f"{name}_proj_b"):
+            project(core, True)
+        for c in range(len(chunks)):
+            with jax.named_scope(f"{name}_ring#s=1#c={c}"):
+                arrive(got.at[:, :, part_of(c)], p_s.at[c], p_r.at[c], {"kv": partner})
+                pass_on(c, lax.rem(y + far, n_y), [], 0, 2 * way(c))
+                for sign in (1, -1):
+                    pass_on(c, lax.rem(y + n_y + sign * short, n_y), [], slot_of(sign, 1), sign)
+        for step in range(2, short + 1):
+            for c in range(len(chunks)):
+                with jax.named_scope(f"{name}_ring#s={step}#c={c}"):
+                    for sign in (-way(c), way(c)):
+                        received = [slot_of(sign, step - 1)]
+                        if step == 2 and sign == way(c):
+                            received.append(0)
+                        for slot in received:
+                            take(c, slot)
+                        dest = lax.rem(y + n_y + sign * (short + 1 - step), n_y)
+                        pass_on(c, dest, received, slot_of(sign, step), sign)
+
+        def finish(c):
+            received = [slot_of(sign, short) for sign in (1, -1)]
+            for slot in received:
+                take(c, slot)
+            return [value for _, _, value in add_up(c, y, received)]
+
+        return finish
 
     def gather_over_kv(buffer, sems):
         r_s, r_r, f_s, f_r = sems
@@ -250,30 +279,27 @@
             total = total + into[d].astype(F32)
         return total
 
-    z_total = z1_own.at[y]
     x_raw[...] = token_t[...].T.reshape(x_raw.shape)
-    reduce_over_kv(
-        norm_gain, w1, n_main, 2 * heads, True, z1_pair, z1_own, z1_got, z1_send, z1_recv, (p1_s, p1_r, a_s, a_r), z_total
+    sums = sum_over_kv(
+        "in", norm_gain, w1, 2 * heads, with_ends([[LANES, dq, dk], [dv], [dv]]),
+        z1_pair, z1_own, z1_got, z1_send, z1_recv, (p1_s, p1_r, a_s, a_r),
     )
-    with jax.named_scope("gates"):
-        gates = tile_of(z_total, z1_recv, n_main)
-        scale1 = lax.rsqrt(gates[:, 2 * heads : 2 * heads + 1] / n_feats + 1e-06)
-        query = scale1 * total_of(z_total, z1_recv, 0, dq) * DQK ** (-0.5)
-        key = scale1 * total_of(z_total, z1_recv, dq, dk)
-        value = scale1 * total_of(z_total, z1_recv, dq + dk, dv)
-        outgate = scale1 * total_of(z_total, z1_recv, dq + dk + dv, dv)
-        igate = scale1 * gates[:, :heads]
-        forget = scale1 * gates[:, heads : 2 * heads]
-        lforget = jnp.minimum(forget, 0.0) - jnp.log1p(jnp.exp(-jnp.abs(forget)))
-        loads["stab"].wait()
-        loads["norm"].wait()
-        loads["mem"].wait()
-        held = lforget + stab[...].T
-        new_stab = jnp.maximum(held, igate)
-        newstab_ref[...] = new_stab.T
-        decay = jnp.exp(held - new_stab)
-        inflow = jnp.exp(igate - new_stab)
-        floor = jnp.exp(-new_stab)
+    gates, query, key = sums(0)
+    scale1 = lax.rsqrt(gates[:, 2 * heads : 2 * heads + 1] / n_feats + 1e-06)
+    query = scale1 * query * DQK ** (-0.5)
+    key = scale1 * key
+    igate = scale1 * gates[:, :heads]
+    forget = scale1 * gates[:, heads : 2 * heads]
+    lforget = jnp.minimum(forget, 0.0) - jnp.log1p(jnp.exp(-jnp.abs(forget)))
+    loads["stab"].wait()
+    loads["norm"].wait()
+    loads["mem"].wait()
+    held = lforget + stab[...].T
+    new_stab = jnp.maximum(held, igate)
+    newstab_ref[...] = new_stab.T
+    decay = jnp.exp(held - new_stab)
+    inflow = jnp.exp(igate - new_stab)
+    floor = jnp.exp(-new_stab)
     with jax.named_scope("readout"):
         query_t = query.T
         for s in range(own):
@@ -281,15 +307,26 @@
                 column = query_t[h * DQK : (h + 1) * DQK, s : s + 1]
                 numer[s : s + 1, h * DV : (h + 1) * DV] = jnp.sum(column * mem[s, h], axis=0, keepdims=True)
     with jax.named_scope("norm"):
+        parts = []
         for h in range(heads):
             q, k = query[:, h * DQK : (h + 1) * DQK], key[:, h * DQK : (h + 1) * DQK]
             keep, add = decay[:, h : h + 1], inflow[:, h : h + 1]
             new_norm = keep * norm[:, h, :] + add * k
             newnorm_ref[:, h, :] = new_norm
             denom = jnp.maximum(jnp.abs(jnp.sum(q * new_norm, axis=1, keepdims=True)), floor[:, h : h + 1])
+            parts.append((keep * numer[:, h * DV : (h + 1) * DV], add * jnp.sum(q * k, axis=1, keepdims=True), denom))
+    with jax.named_scope("value"):
+        (value,) = sums(1)
+        value = scale1 * value
+        readout = [
+            (top + weight * value[:, h * DV : (h + 1) * DV]) / denom for h, (top, weight, denom) in enumerate(parts)
+        ]
+    with jax.named_scope("outgate"):
+        (outgate,) = sums(2)
+        outgate = scale1 * outgate
+        for h in range(heads):
             at = slice(h * DV, (h + 1) * DV)
-            top = keep * numer[:, at] + (add * jnp.sum(q * k, axis=1, keepdims=True)) * value[:, at]
-            gated[rows(kv, own), at] = (jax.nn.sigmoid(outgate[:, at]) * (top / denom)).astype(BF16)
+            gated[rows(kv, own), at] = (jax.nn.sigmoid(outgate[:, at]) * readout[h]).astype(BF16)
     finish = gather_over_kv(gated, (g_s, g_r, gf_s, gf_r))
 
     with jax.named_scope("newmem"):
@@ -322,109 +359,19 @@
 
     x_raw[...] = mixed_t[...].T.reshape(x_raw.shape)
     chunks = ff_chunks(n_ff)
-    order = [len(chunks) - 1] + list(range(len(chunks) - 1))
-    wide_lane = lax.broadcasted_iota(jnp.int32, (half_rows, LANES), 1)
-    small_lane = lax.broadcasted_iota(jnp.int32, (own, LANES), 1)
-
-    def project_chunks(core_of, ours):
-        wide = x_raw[:, core_of].reshape(half_rows, feats).astype(F32)
-        normed = (wide * ffn_gain[...].astype(F32)[None, :]).astype(BF16)
-        squares = jnp.sum(wide * wide, axis=1, keepdims=True)
-        tile = jnp.broadcast_to(squares, (half_rows, LANES))
-        if ours:
-            z2_own[:, :, 2 * n_ff :] = tile.reshape(n_y, own, LANES)
-        else:
-            z2_pair[:, :, 2 * n_ff :] = hi_lo(tile, wide_lane).reshape(n_y, own, LANES)
-        for c in order:
-            at, size = chunks[c]
-            for start in (2 * at, 2 * at + size):
-                z = jnp.dot(normed, w2[:, start : start + size], preferred_element_type=F32)
-                if ours:
-                    z2_own[:, :, start : start + size] = z.reshape(n_y, own, size)
-                else:
-                    z2_pair[:, :, start : start + size] = z.astype(BF16).reshape(n_y, own, size)
-            if not ours:
-                part = pl.ds(2 * at, width_of(c))
-                send(z2_pair.at[:, :, part], z2_got.at[:, :, part], p2_s.at[c], p2_r.at[c], {"kv": partner})
-
-    def width_of(c):
-        return 2 * chunks[c][1] + (LANES if c == len(chunks) - 1 else 0)
-
-    def spans(c):
-        at, size = chunks[c]
-        return [(2 * at, size, False), (2 * at + size, size, False)] + (
-            [(2 * n_ff, LANES, True)] if c == len(chunks) - 1 else []
-        )
-
-    def plain(tile, is_square):
-        tile = tile.astype(F32)
-        if is_square:
-            tile = tile + jnp.concatenate([tile[:, HALF:], tile[:, :HALF]], axis=1)
-        return tile
-
-    def add_up(c, dest, received, put):
-        for at, size, is_square in spans(c):
-            value = z2_own[dest, :, at : at + size] + plain(z2_got[dest, :, at : at + size], is_square)
-            for slot in received:
-                value = value + plain(z2_recv[slot, :, at : at + size], is_square)
-            put(at, size, is_square, value)
-
-    def pass_on(c, dest, received, slot, hops):
-        def put(at, size, is_square, value):
-            z2_send[slot, :, at : at + size] = hi_lo(value, small_lane) if is_square else value.astype(BF16)
-
-        add_up(c, dest, received, put)
-        part = pl.ds(2 * chunks[c][0], width_of(c))
-        where = {"kv": 2 * lax.rem(y + n_y + hops, n_y) + core}
-        send(z2_send.at[slot, :, part], z2_recv.at[slot, :, part], b_s.at[slot, c], b_r.at[slot, c], where)
-
-    def take(c, slot):
-        part = pl.ds(2 * chunks[c][0], width_of(c))
-        target = z2_recv.at[slot, :, part]
-        arrive(target, b_s.at[slot, c], b_r.at[slot, c], {"kv": partner})
-
-    far, short = n_y // 2, n_y // 2 - 1
-    with jax.named_scope("proj2a"):
-        project_chunks(other, False)
-    with jax.named_scope("proj2b"):
-        project_chunks(core, True)
-
-    def way(c):
-        return 1 if c % 2 == 0 else -1
-
-    def slot_of(sign, step):
-        return step if sign == 1 else short + step
-
-    for c in order:
-        with jax.named_scope(f"ring#s=1#c={c}"):
-            part = pl.ds(2 * chunks[c][0], width_of(c))
-            arrive(z2_got.at[:, :, part], p2_s.at[c], p2_r.at[c], {"kv": partner})
-            pass_on(c, lax.rem(y + far, n_y), [], 0, 2 * way(c))
-            for sign in (1, -1):
-                pass_on(c, lax.rem(y + n_y + sign * short, n_y), [], slot_of(sign, 1), sign)
-    for step in range(2, short + 1):
-        for c in order:
-            with jax.named_scope(f"ring#s={step}#c={c}"):
-                for sign in (-way(c), way(c)):
-                    received = [slot_of(sign, step - 1)]
-                    if step == 2 and sign == way(c):
-                        received.append(0)
-                    for slot in received:
-                        take(c, slot)
-                    pass_on(c, lax.rem(y + n_y + sign * (short + 1 - step), n_y), received, slot_of(sign, step), sign)
+    sizes = [[size, size] for _, size in chunks]
+    sizes[0] = [LANES] + sizes[0]
+    sums = sum_over_kv(
+        "ff", ffn_gain, w2, None, with_ends(sizes), z2_pair, z2_own, z2_got, z2_send, z2_recv, (p2_s, p2_r, b_s, b_r)
+    )
 
     scale2 = None
-    for c in order:
-        at, size = chunks[c]
+    for c, (at, size) in enumerate(chunks):
         with jax.named_scope(f"hidden#c={c}"):
-            parts = []
-            received = [slot_of(sign, short) for sign in (1, -1)]
-            for slot in received:
-                take(c, slot)
-            add_up(c, y, received, lambda at, size, is_square, value: parts.append(value))
-            if scale2 is None:
-                scale2 = lax.rsqrt(parts[2][:, :1] / n_feats + 1e-06)
-            gate, up = scale2 * parts[0], scale2 * parts[1]
+            *squares, gate, up = sums(c)
+            if c == 0:
+                scale2 = lax.rsqrt(squares[0][:, :1] / n_feats + 1e-06)
+            gate, up = scale2 * gate, scale2 * up
             hidden[rows(kv, own), at : at + size] = (gate * jax.nn.sigmoid(gate) * up).astype(BF16)
             part = hidden.at[rows(kv, own), pl.ds(at, size)]
             for d in far_first(n_y):
@@ -449,14 +396,14 @@
                 wd_t[:, at : at + size], hidden[:, at : at + size], (((1,), (1,)), ((), ())), preferred_element_type=F32
             )
 
-    pass_to_partner(order[0])
-    for i, c in enumerate(order):
-        if i + 1 < len(order):
-            pass_to_partner(order[i + 1])
+    pass_to_partner(0)
+    for c in range(len(chunks)):
+        if c + 1 < len(chunks):
+            pass_to_partner(c + 1)
         product = down_part(c)
-        if i == 0:
+        if c == 0:
             down_sum[...] = product
-        elif i + 1 < len(order):
+        elif c + 1 < len(chunks):
             down_sum[...] += product
     with jax.named_scope("downrs"):
         total = sum_over_tp(down_sum[...] + product, down_send, down_recv, (d_s, d_r))
@@ -516,7 +463,7 @@
     vmem = pl.BlockSpec(memory_space=pltpu.VMEM)
     dma = pltpu.SemaphoreType.DMA
     n_chunks = len(ff_chunks(n_ff))
-    ys, xs, one, per_chunk = dma((n_y,)), dma((n_tp,)), dma, dma((n_y, n_chunks))
+    ys, xs, per_chunk = dma((n_y,)), dma((n_tp,)), dma((n_y, n_chunks))
     out_t, new_memory, new_normalizer, new_stabilizer = pl.pallas_call(
         functools.partial(layer_kernel, n_kv, n_tp),
         out_shape=(
@@ -535,7 +482,7 @@
             pltpu.VMEM(stabilizer.shape[::-1], F32),
             pltpu.VMEM(w_mix_out.shape, BF16),
             pltpu.VMEM(w_mix_out.shape[::-1], BF16),
-            pltpu.VMEM((feats, 2 * n_ff), BF16),
+            pltpu.VMEM((feats, n2), BF16),
             pltpu.VMEM(w_down.shape, BF16),
             pltpu.VMEM(w_down.shape[::-1], BF16),
             pltpu.VMEM((feats, seqs), BF16),
@@ -561,7 +508,7 @@
             pltpu.VMEM((n_tp, mine, seqs), BF16),
             dma((13 + 2 * len(ff_chunks(n_ff)),)),
             xs, xs,
-            one, one, ys, ys,
+            dma((3,)), dma((3,)), dma((n_y, 3)), dma((n_y, 3)),
             ys, ys, ys, ys,
             xs, xs,
             xs, xs,

time: 95.7 us -> 94.9 us (level)
  no operation moved by 1% of the time
where the time goes in v4:
time: 94.9 us; the launch traced here: 94.6 us
  Pallas kernels  93.9 us (99%)
    pallas_call x1, Pallas kernels, shards(): pl.pallas_call(functools.partial(layer_kernel, n_kv, n_tp), out_shape=(ja...  91.4 us
    pallas_call x1, Pallas kernels, hand_over(): pl.pallas_call(functools.partial(copy_kernel, pieces), out_shape=tuple((j...  2.5 us

profile of v4, /device:TPU:513, one launch (start us, length us, event | category | flops | bytes accessed | tf_op | source)
XLA Modules:
  0.0 94.6 jit_solution(12126324561498105640)
XLA Ops:
  0.6 91.4 %layer.1 = (bf16[32,256]{1,0:T(8,128)(2,1)}, f32[16,4,64,128]{3,2,1,0:T(8,128)}, f32[16,4,64]{2,1,0:T(4,128)}, f32[4,16]{1,0:T(4,128)}) custom-call(bf16[32,256]{1,0:T(8,128)(2,1)} %bitcast.6, bf16[256]{0:T(256)(128)(2,1)} %norm_gain.1, bf16[256,256]{1,0:T(8,128)(2,1)} %wq_h.1, bf16[256,256]{1,0:T(8,128)(2,1)} %wk_h.1, bf16[256,512]{1,0:T(8,128)(2,1)} %wv_h.1, ...), custom_call_target="tpu_custom_call" | custom-call | tf_op jit(solution)/shard_map/layer/pallas_call | solution.py:467
  92.1 2.5 %hand_over.1 = (bf16[32,256]{1,0:T(8,128)(2,1)}, f32[16,4,64,128]{3,2,1,0:T(8,128)}, f32[16,4,64]{2,1,0:T(4,128)}, f32[4,16]{1,0:T(4,128)}) custom-call(bf16[32,256]{1,0:T(8,128)(2,1)} %get-tuple-element.12.refs_0_, f32[16,4,64,128]{3,2,1,0:T(8,128)} %get-tuple-element.13.refs_1_, f32[16,4,64]{2,1,0:T(4,128)} %get-tuple-element.14.refs_2_, ...), custom_call_target="tpu_custom_call" | custom-call | tf_op jit(solution)/shard_map/hand_over/pallas_call | solution.py:441
